TPU v7x, 32 devices: a whole 2x2x4 slice. The times are simulated.
32 devices in a mesh: sp: 8 (over z, y), tp: 4 (over x, core).
Axes of the slice: x: 2, y: 2, z: 4, core: 2. Of those that a mesh axis runs over, the one named last changes fastest.
Arguments:
- grad_out: bfloat16 [2048, 2048], P('sp'), may hold values from -6 to 6
- resid: bfloat16 [2048, 2048], P('sp'), may hold values from -6 to 6
- norm_gain: float32 [2048], replicated, may hold values from 0.1 to 1.9
- routes: int32 [2048, 2], P('sp'), may hold values from 0 to 7, all different within a row; in each aligned block of 256 rows (0 to 255, 256 to 511, ...) at most 96 rows name the same one
- route_weights: float32 [2048, 2], P('sp'), may hold values from 0.05 to 1
- gate_weight: bfloat16 [8, 2048, 1536], P('sp', None, 'tp'), may hold values from -0.375 to 0.375
- up_weight: bfloat16 [8, 2048, 1536], P('sp', None, 'tp'), may hold values from -0.375 to 0.375
- down_weight: bfloat16 [8, 1536, 2048], P('sp', 'tp'), may hold values from -0.15625 to 0.15625
- proj_weight: bfloat16 [2048, 512], P(None, 'tp'), may hold values from -0.25 to 0.25
- conv_sum: bfloat16 [2048, 512], P('sp', 'tp'), may hold values from -6 to 6
- conv_gain: float32 [512], P('tp'), may hold values from 0.1 to 1.9
- conv_taps: float32 [31, 512], P(None, 'tp'), may hold values from -1 to 1
- conv_value: bfloat16 [2048, 512], P('sp', 'tp'), may hold values from -6 to 6
- conv_gate: bfloat16 [2048, 512], P('sp', 'tp'), may hold values from -6 to 6
Outputs:
- gate_weight_grad: bfloat16 [8, 2048, 1536], P('sp', None, 'tp')
- up_weight_grad: bfloat16 [8, 2048, 1536], P('sp', None, 'tp')
- down_weight_grad: bfloat16 [8, 1536, 2048], P('sp', 'tp')
- proj_grad: float32 [2048, 512], P('sp', 'tp')
- value_grad: bfloat16 [2048, 512], P('sp', 'tp')
- gate_input_grad: bfloat16 [2048, 512], P('sp', 'tp')
Inputs may be any that keep to these rules, and one draw needn't show every extreme that they name: In each aligned block of 256 tokens no expert is named by more than 96 routes, and in some block one expert is named exactly 96 times; a token's two routes name different experts.
All inputs are finite; a program needn't handle non-finite values.
Results may differ from a plain program's by a relative error of at most 0.028.
Values may be sent and summed in bfloat16 or wider, within the bound.
A program may use at most 128 MiB of HBM per device.

v0:
```python
import functools

import jax
import jax.numpy as jnp
from jax import lax
from jax.experimental import pallas as pl
from jax.experimental.pallas import tpu as pltpu
from jax.sharding import PartitionSpec as P

CONV_K = 31
GROUP = 128
MESH = pl.DeviceIdType.MESH


CLAMP_LIMIT = 7.0
SLOPE_ALPHA = 1.702


def passed_along(block, axis, distance):
    devices = range(lax.axis_size(axis))
    route = [(i - distance, i) for i in devices if i - distance in devices]
    return lax.ppermute(block, axis, route)


def tp_places():
    mine = lax.axis_index("tp")
    near = mine + 1 - 2 * (mine % 2)
    far = (mine + 2) % 4
    diag = (near + 2) % 4
    return mine, near, far, diag


def meet(steps, over_sp, near, far):
    s, t = lax.axis_index("sp"), lax.axis_index("tp")
    barrier = pltpu.get_barrier_semaphore()
    pl.semaphore_signal(barrier, inc=1, device_id=(s, near), device_id_type=MESH)
    pl.semaphore_signal(barrier, inc=1, device_id=(s, far), device_id_type=MESH)
    total = 2
    if over_sp:

        def greet(d, carry):
            pl.semaphore_signal(
                barrier, inc=1, device_id=((s + d) % steps, t), device_id_type=MESH
            )
            return carry

        lax.fori_loop(1, steps, greet, 0)
        total += steps - 1
    pl.semaphore_wait(barrier, total)


def crossing_first(steps, k):
    return steps // 2 + ((k + 1) // 2) * (2 * (k % 2) - 1)


def looped(first, last, body):
    def step(k, carry):
        body(k)
        return carry

    lax.fori_loop(first, last, step, 0)


def spread_kernel(count, steps, over_sp, in_lanes, absolute, beside, sp_count, *refs):
    refs = list(refs)
    sends, refs = refs[:count], refs[count:]
    fulls, refs = (refs[:count], refs[count:]) if over_sp else (None, refs)
    side, refs = (refs[0], refs[1:]) if beside else (None, refs)
    outs, refs = refs[:count], refs[count:]
    side_out, refs = (refs[0], refs[1:]) if beside else (None, refs)
    own_sem, a_send, a_recv, b_send, f_send, c_send, near_recv, fwd_recv, far_recv = refs[:9]
    s = lax.axis_index("sp")
    t, near, far, _ = tp_places()
    width = sends[0].shape[-1]

    def place(c, d, q):
        if in_lanes:
            return outs[c].at[d, :, pl.ds(pl.multiple_of(q * width, width), width)]
        return outs[c].at[d, q]

    def source(c, d):
        return sends[c].at[(s + d) % steps if absolute else d]

    def own(c, d):
        if over_sp:
            return pltpu.make_async_copy(fulls[c], outs[c].at[0], own_sem.at[c, 0])
        return pltpu.make_async_copy(source(c, d), place(c, d, t), own_sem.at[c, d])

    def to_sp(c, d):
        return pltpu.make_async_remote_copy(
            src_ref=source(c, d),
            dst_ref=place(c, d, t),
            send_sem=a_send.at[c, d],
            recv_sem=a_recv.at[c, d],
            device_id=((s + d) % steps, t),
            device_id_type=MESH,
        )

    def to_tp(c, d, q, target, send_sem, recv_sem):
        return pltpu.make_async_remote_copy(
            src_ref=place(c, d, q),
            dst_ref=place(c, d, q),
            send_sem=send_sem.at[c, d],
            recv_sem=recv_sem.at[c, d],
            device_id=(s, target),
            device_id_type=MESH,
        )

    def near_copy(c, d):
        return to_tp(c, d, t, near, b_send, near_recv)

    def far_copy(c, d):
        return to_tp(c, d, t, far, f_send, far_recv)

    def fwd_copy(c, d):
        return to_tp(c, d, far, near, c_send, fwd_recv)

    def side_copy(d):
        side_send, side_recv = refs[10:12]
        return pltpu.make_async_remote_copy(
            src_ref=side,
            dst_ref=side_out.at[d],
            send_sem=side_send.at[d],
            recv_sem=side_recv.at[d],
            device_id=((s + d) % sp_count, t),
            device_id_type=MESH,
        )

    def own_side():
        return pltpu.make_async_copy(side, side_out.at[0], refs[9].at[0])

    def share(c, d):
        far_copy(c, d).start()
        near_copy(c, d).start()

    def forward(c, d):
        far_copy(c, d).wait_recv()
        fwd_copy(c, d).start()

    def finish(c, d):
        near_copy(c, d).wait()
        far_copy(c, d).wait_send()
        fwd_copy(c, d).wait()

    def loop(first, last, body):
        def each(k):
            d = k + 1 if over_sp else k
            for c in range(count):
                body(c, d)

        looped(first, last, each)

    meet(sp_count, over_sp or beside, near, far)
    if over_sp:
        loop(0, steps - 1, lambda c, d: to_sp(c, d).start())
        for c in range(count):
            own(c, 0).start()

        def pass_on(k):
            for c in range(count):
                d = k + 1
                to_sp(c, d).wait_recv()
                share(c, d)

        def pass_on_twice(k):
            pass_on(k)
            for c in range(count):
                forward(c, k)

        pass_on(0)
        looped(1, steps - 1, pass_on_twice)
        loop(steps - 2, steps - 1, forward)
        loop(0, steps - 1, finish)
        loop(0, steps - 1, lambda c, d: to_sp(c, d).wait_send())
        for c in range(count):
            own(c, 0).wait()
    else:
        loop(0, steps, lambda c, d: own(c, d).start())
        if beside:
            looped(0, sp_count - 1, lambda k: side_copy(crossing_first(sp_count, k)).start())
            own_side().start()

        def share_own(c, d):
            own(c, d).wait()
            share(c, d)

        loop(0, steps, share_own)
        loop(0, steps, forward)
        loop(0, steps, finish)
        if beside:
            looped(0, sp_count - 1, lambda k: side_copy(crossing_first(sp_count, k)).wait())
            own_side().wait()


def spread(sends, fulls, side, in_lanes, absolute, collective_id):
    count = len(sends)
    steps, rows, width = sends[0].shape
    tp_count, sp_count = lax.axis_size("tp"), lax.axis_size("sp")
    over_sp, beside = fulls is not None, side is not None
    shape = (steps, rows, tp_count * width) if in_lanes else (steps, tp_count, rows, width)
    out_shape = [jax.ShapeDtypeStruct(shape, x.dtype) for x in sends]
    operands = list(sends) + (list(fulls) if over_sp else []) + ([side] if beside else [])
    scratch = [pltpu.SemaphoreType.DMA((count, steps))] * 9
    if beside:
        out_shape.append(jax.ShapeDtypeStruct((sp_count,) + side.shape, side.dtype))
        scratch += [pltpu.SemaphoreType.DMA((1,))] + [pltpu.SemaphoreType.DMA((sp_count,))] * 2
    return pl.pallas_call(
        functools.partial(
            spread_kernel, count, steps, over_sp, in_lanes, absolute, beside, sp_count
        ),
        out_shape=tuple(out_shape),
        in_specs=[pl.BlockSpec(memory_space=pltpu.VMEM)] * len(operands),
        out_specs=tuple(pl.BlockSpec(memory_space=pltpu.VMEM) for _ in out_shape),
        scratch_shapes=scratch,
        compiler_params=pltpu.CompilerParams(
            collective_id=collective_id, has_side_effects=True, vmem_limit_bytes=40 << 20
        ),
    )(*operands)


def combine_kernel(
    steps, part, out, near_in, pair, far_in, total,
    n0_send, n0_recv, n1_send, n1_recv, f_send, f_recv, a_send, a_recv,
):
    s = lax.axis_index("sp")
    t, near, far, diag = tp_places()
    width = out.shape[-1]

    def lanes(q):
        return pl.ds(pl.multiple_of(q * width, width), width)

    def near_copy(d, which, q, send_sem, recv_sem):
        return pltpu.make_async_remote_copy(
            src_ref=part.at[d, :, lanes(q)],
            dst_ref=near_in.at[which, d],
            send_sem=send_sem.at[d],
            recv_sem=recv_sem.at[d],
            device_id=(s, near),
            device_id_type=MESH,
        )

    def for_near(d):
        return near_copy(d, 0, near, n0_send, n0_recv)

    def for_diag(d):
        return near_copy(d, 1, diag, n1_send, n1_recv)

    def far_copy(d):
        return pltpu.make_async_remote_copy(
            src_ref=pair.at[d],
            dst_ref=far_in.at[d],
            send_sem=f_send.at[d],
            recv_sem=f_recv.at[d],
            device_id=(s, far),
            device_id_type=MESH,
        )

    def back(d):
        return pltpu.make_async_remote_copy(
            src_ref=total.at[d],
            dst_ref=out.at[d],
            send_sem=a_send.at[d],
            recv_sem=a_recv.at[d],
            device_id=((s + steps - d) % steps, t),
            device_id_type=MESH,
        )

    meet(steps, True, near, far)

    def open_up(d):
        for_diag(d).start()
        for_near(d).start()

    def add_pair(d):
        for_diag(d).wait_recv()
        mine = part[d, :, lanes(far)].astype(jnp.float32)
        pair[d] = (mine + near_in[1, d].astype(jnp.float32)).astype(pair.dtype)
        far_copy(d).start()

    def whole(d):
        for_near(d).wait_recv()
        far_copy(d).wait_recv()
        mine = part[d, :, lanes(t)].astype(jnp.float32)
        both = mine + near_in[0, d].astype(jnp.float32)
        return (both + far_in[d].astype(jnp.float32)).astype(out.dtype)

    def send_back(d):
        total[d] = whole(d)
        back(d).start()

    def at(k):
        return crossing_first(steps, k)

    lag = min(3, steps - 1)
    looped(0, steps - 1, lambda k: open_up(at(k)))
    open_up(0)
    looped(0, lag, lambda k: add_pair(at(k)))

    def middle(k):
        add_pair(at(k))
        send_back(at(k - lag))

    looped(lag, steps - 1, middle)
    add_pair(0)
    looped(steps - 1 - lag, steps - 1, lambda k: send_back(at(k)))
    out[0] = whole(0)

    def finish(d):
        for_near(d).wait_send()
        for_diag(d).wait_send()
        far_copy(d).wait_send()

    looped(0, steps, finish)
    looped(1, steps, lambda d: back(d).wait())


def combine(part, collective_id):
    steps, rows, all_width = part.shape
    width = all_width // lax.axis_size("tp")
    block = (steps, rows, width)
    return pl.pallas_call(
        functools.partial(combine_kernel, steps),
        out_shape=jax.ShapeDtypeStruct(block, part.dtype),
        in_specs=[pl.BlockSpec(memory_space=pltpu.VMEM)],
        out_specs=pl.BlockSpec(memory_space=pltpu.VMEM),
        scratch_shapes=[
            pltpu.VMEM((2,) + block, part.dtype),
            pltpu.VMEM(block, part.dtype),
            pltpu.VMEM(block, part.dtype),
            pltpu.VMEM(block, part.dtype),
        ]
        + [pltpu.SemaphoreType.DMA((steps,))] * 8,
        compiler_params=pltpu.CompilerParams(
            collective_id=collective_id, has_side_effects=True, vmem_limit_bytes=40 << 20
        ),
    )(part)


def contract_rows(left_side, right_side):
    return lax.dot_general(
        left_side, right_side, (((0,), (0,)), ((), ())), preferred_element_type=jnp.float32
    )


def contract_cols(left_side, right_side):
    return lax.dot_general(
        left_side, right_side, (((1,), (1,)), ((), ())), preferred_element_type=jnp.float32
    )


def expert_backward(routed_rows, routed_cots, w_gate, w_up, w_down):
    gate_pre = jnp.dot(routed_rows, w_gate, preferred_element_type=jnp.float32)
    up_pre = jnp.dot(routed_rows, w_up, preferred_element_type=jnp.float32)
    gate_clamped = jnp.minimum(gate_pre, CLAMP_LIMIT)
    up_clamped = jnp.clip(up_pre, -CLAMP_LIMIT, CLAMP_LIMIT)
    sigma = jax.nn.sigmoid(SLOPE_ALPHA * gate_clamped)
    gated = gate_clamped * sigma
    act = ((up_clamped + 1.0) * gated).astype(jnp.bfloat16)
    down_grad = contract_rows(act, routed_cots).astype(jnp.bfloat16)
    act_grad = contract_cols(routed_cots, w_down)
    inside = (up_pre > -CLAMP_LIMIT) & (up_pre < CLAMP_LIMIT)
    up_pre_grad = jnp.where(inside, act_grad * gated, 0.0).astype(jnp.bfloat16)
    slope = sigma + SLOPE_ALPHA * gate_clamped * sigma * (1.0 - sigma)
    gate_pre_grad = jnp.where(
        gate_pre < CLAMP_LIMIT, act_grad * (up_clamped + 1.0) * slope, 0.0
    ).astype(jnp.bfloat16)
    gate_grad = contract_rows(routed_rows, gate_pre_grad).astype(jnp.bfloat16)
    up_grad = contract_rows(routed_rows, up_pre_grad).astype(jnp.bfloat16)
    partial_value = contract_cols(gate_pre_grad, w_gate) + contract_cols(up_pre_grad, w_up)
    return (gate_grad, up_grad, down_grad, partial_value)


def local(
    grad_out,
    resid,
    norm_gain,
    routes,
    route_weights,
    gate_weight,
    up_weight,
    down_weight,
    proj_weight,
    conv_sum,
    conv_gain,
    conv_taps,
    conv_value,
    conv_gate,
):
    tok_rows, model_width = resid.shape
    sp_count = lax.axis_size("sp")
    tp_count = lax.axis_size("tp")
    capacity = 3 * tok_rows // sp_count
    col_count = model_width // tp_count
    resid_f = resid.astype(jnp.float32)
    inv_rms = lax.rsqrt(jnp.mean(resid_f * resid_f, axis=-1, keepdims=True) + 1e-06)
    normed = (resid_f * inv_rms * norm_gain).astype(jnp.bfloat16)
    my_sp = lax.axis_index("sp")
    away = (routes - my_sp) % sp_count
    steps_away = jnp.arange(sp_count, dtype=jnp.int32)
    named = away[:, :, None] == steps_away[None, None, :]
    chosen = jnp.any(named, axis=1)
    weight_of = jnp.sum(jnp.where(named, route_weights[:, :, None], 0.0), axis=1)
    token_ids = jnp.arange(tok_rows, dtype=jnp.int32)
    earlier = (token_ids[None, :] < token_ids[:, None]).astype(jnp.bfloat16)
    rank = jnp.dot(earlier, chosen.astype(jnp.bfloat16), preferred_element_type=jnp.float32)
    rank = jnp.where(chosen, rank, -1.0).astype(jnp.int32)
    slots = jnp.arange(capacity, dtype=jnp.int32)
    held = rank.T[:, None, :] == slots[None, :, None]
    slot_weight = jnp.sum(jnp.where(held, weight_of.T[:, None, :], 0.0), axis=2)
    pick = held.astype(jnp.bfloat16).reshape(sp_count * capacity, tok_rows)
    first_col = lax.axis_index("tp") * col_count
    normed_part = lax.dynamic_slice_in_dim(normed, first_col, col_count, 1)
    cots_part = lax.dynamic_slice_in_dim(grad_out, first_col, col_count, 1)
    slot_weight = slot_weight.reshape(-1, 1)
    send_rows = jnp.dot(pick, normed_part, preferred_element_type=jnp.float32).astype(jnp.bfloat16)
    send_cots = jnp.dot(pick, cots_part, preferred_element_type=jnp.float32)
    send_cots = (send_cots * slot_weight).astype(jnp.bfloat16)
    own_pick = pick[:capacity]
    own_rows = jnp.dot(own_pick, normed, preferred_element_type=jnp.float32).astype(jnp.bfloat16)
    own_cots = jnp.dot(own_pick, grad_out, preferred_element_type=jnp.float32)
    own_cots = (own_cots * slot_weight[:capacity]).astype(jnp.bfloat16)
    routed_rows, routed_cots = spread(
        (
            send_rows.reshape(sp_count, capacity, col_count),
            send_cots.reshape(sp_count, capacity, col_count),
        ),
        (own_rows, own_cots),
        None,
        True,
        False,
        0,
    )
    routed_rows = routed_rows.reshape(sp_count * capacity, model_width)
    routed_cots = routed_cots.reshape(sp_count * capacity, model_width)
    gate_grad, up_grad, down_grad, partial_value = expert_backward(
        routed_rows, routed_cots, gate_weight[0], up_weight[0], down_weight[0]
    )
    returned = combine(
        partial_value.reshape(sp_count, capacity, model_width).astype(jnp.bfloat16), 1
    ).reshape(sp_count * capacity, col_count)
    normed_part_grad = contract_rows(pick, returned).astype(jnp.bfloat16)
    channels = conv_sum.shape[1]
    summed = conv_sum.astype(jnp.float32).reshape(tok_rows, channels // GROUP, GROUP)
    centre = summed - jnp.mean(summed, axis=-1, keepdims=True)
    inv_std = lax.rsqrt(jnp.mean(centre * centre, axis=-1, keepdims=True) + 1e-05)
    grouped = centre * inv_std
    chan_normed = grouped.reshape(tok_rows, channels)
    pre_act = chan_normed * conv_gain
    sigma_conv = jax.nn.sigmoid(pre_act)
    conv_out = (pre_act * sigma_conv).astype(jnp.bfloat16)
    chunks = 4
    normed_grad, all_out = spread(
        (normed_part_grad.reshape(chunks, tok_rows // chunks, col_count),),
        None,
        conv_out,
        True,
        False,
        2,
    )
    normed_grad = normed_grad.reshape(tok_rows, model_width)
    feature_grad = normed_grad.astype(jnp.float32) * norm_gain
    cubed = inv_rms * inv_rms * inv_rms
    resid_grad = (
        grad_out.astype(jnp.float32)
        + inv_rms * feature_grad
        - resid_f * cubed * jnp.mean(resid_f * feature_grad, axis=-1, keepdims=True)
    ).astype(jnp.bfloat16)
    share = tok_rows // tp_count
    feat_rows = model_width // sp_count
    tokens_part = lax.dynamic_slice_in_dim(resid_grad, lax.axis_index("tp") * share, share, 0)
    by_feature = tokens_part.reshape(share, sp_count, feat_rows).transpose(1, 0, 2)
    own_features = lax.dynamic_slice_in_dim(resid_grad, my_sp * feat_rows, feat_rows, 1)
    (feature_cols,) = spread(
        (by_feature,), (own_features.reshape(tp_count, share, feat_rows),), None, False, True, 3
    )
    proj_grad = contract_rows(
        feature_cols.reshape(sp_count * tok_rows, feat_rows),
        all_out.reshape(sp_count * tok_rows, channels),
    )
    out_grad = jnp.dot(resid_grad, proj_weight, preferred_element_type=jnp.float32)
    normal_grad = (
        out_grad * sigma_conv * (1.0 + pre_act * (1.0 - sigma_conv)) * conv_gain
    ).reshape(tok_rows, channels // GROUP, GROUP)
    sum_grad = inv_std * (
        normal_grad
        - jnp.mean(normal_grad, axis=-1, keepdims=True)
        - grouped * jnp.mean(normal_grad * grouped, axis=-1, keepdims=True)
    )
    sum_grad = sum_grad.reshape(tok_rows, channels)
    following = passed_along(sum_grad[: CONV_K - 1], "sp", -1)
    extended = jnp.concatenate([sum_grad, following], axis=0)
    gated_grad = lax.conv_general_dilated(
        extended[None],
        conv_taps[::-1][:, None, :],
        (1,),
        ((0, 0),),
        dimension_numbers=("NWC", "WIO", "NWC"),
        feature_group_count=channels,
        precision=lax.Precision.HIGHEST,
    )[0]
    sigma_gate = jax.nn.sigmoid(conv_gate.astype(jnp.float32))
    value_grad = (gated_grad * sigma_gate).astype(jnp.bfloat16)
    gate_input_grad = (
        gated_grad * conv_value.astype(jnp.float32) * sigma_gate * (1.0 - sigma_gate)
    ).astype(jnp.bfloat16)
    return (gate_grad[None], up_grad[None], down_grad[None], proj_grad, value_grad, gate_input_grad)


def solution(mesh):
    in_specs = (
        P("sp", None),
        P("sp", None),
        P(),
        P("sp", None),
        P("sp", None),
        P("sp", None, "tp"),
        P("sp", None, "tp"),
        P("sp", "tp", None),
        P(None, "tp"),
        P("sp", "tp"),
        P("tp"),
        P(None, "tp"),
        P("sp", "tp"),
        P("sp", "tp"),
    )
    out_specs = (
        P("sp", None, "tp"),
        P("sp", None, "tp"),
        P("sp", "tp", None),
        P("sp", "tp"),
        P("sp", "tp"),
        P("sp", "tp"),
    )
    return jax.shard_map(local, mesh=mesh, in_specs=in_specs, out_specs=out_specs, check_vma=False)
```

profile of v0, /device:TPU:0, one launch (start us, length us, event | category | flops | bytes accessed | tf_op | source)
XLA Modules:
  0.0 162.3 jit_solution(4220510499112708132)
XLA Ops:
  0.7 0.8 and_select_fusion
  1.7 0.7 select_reduce_fusion.1
  3.1 1.5 fusion.4
  4.6 1.3 fusion.6
  5.9 1.6 convolution_convert_fusion.3.refs_2_
  7.5 1.3 convolution_convert_fusion.4
  9.6 51.9 %shard_map.181 = (bf16[8,96,2048]{2,1,0:T(8,128)(2,1)S(1)}, bf16[8,96,2048]{2,1,0:T(8,128)(2,1)S(1)}) custom-call(bf16[8,96,512]{2,1,0:T(8,128)(2,1)S(1)} %bitcast.91, bf16[8,96,512]{2,1,0:T(8,128)(2,1)S(1)} %bitcast.92, bf16[96,2048]{1,0:T(8,128)(2,1)S(1)} %convolution_convert_fusion.3.refs_2_, bf16[96,2048]{1,0:T(8,128)(2,1)S(1)} %fusion.3.refs_3_), custom_call_target="tpu_custom_call" | custom-call | tf_op jit(solution)/shard_map/pallas_call | solution.py:207
  61.5 1.8 %fusion.14 = f32[768,384]{1,0:T(8,128)S(1)} fusion(bf16[768,2048]{1,0:T(8,128)(2,1)S(1)} %bitcast.99, bf16[1,2048,384]{2,1,0:T(8,128)(2,1)S(1)} %copy-done.4), kind=kOutput, calls=%fused_computation.25 | convolution fusion | flops 1207959552 | bytes 5898240 | tf_op jit(solution)/shard_map/dot_general | solution.py:353
  63.3 1.8 %fusion.20 = f32[768,384]{1,0:T(8,128)S(1)} fusion(bf16[768,2048]{1,0:T(8,128)(2,1)S(1)} %bitcast.100, bf16[1,2048,384]{2,1,0:T(8,128)(2,1)S(1)} %copy-done), kind=kOutput, calls=%fused_computation.31 | convolution fusion | flops 1207959552 | bytes 5898240 | tf_op jit(solution)/shard_map/dot_general | solution.py:352
  65.1 2.5 %select_convert_fusion = (bf16[768,384]{1,0:T(8,128)(2,1)S(1)}, bf16[768,384]{1,0:T(8,128)(2,1)S(1)}) fusion(f32[768,384]{1,0:T(8,128)S(1)} %fusion.14, f32[768,384]{1,0:T(8,128)S(1)} %fusion.20, bf16[768,2048]{1,0:T(8,128)(2,1)S(1)} %bitcast.97, bf16[1,384,2048]{2,1,0:T(8,128)(2,1)S(1)} %copy-done.11), kind=kOutput, calls=%fused_computation.38 | convolution fusion | flops 1214742528 | bytes 8257536 | tf_op jit(solution)/shard_map/dot_general | solution.py:346
  67.6 1.8 %fusion.18 = f32[768,2048]{1,0:T(8,128)S(1)} fusion(bf16[768,384]{1,0:T(8,128)(2,1)S(1)} %get-tuple-element.17, bf16[1,2048,384]{2,1,0:T(8,128)(2,1)S(1)} %copy-done), kind=kOutput, calls=%fused_computation.29 | convolution fusion | flops 1207959552 | bytes 8454144 | tf_op jit(solution)/shard_map/dot_general | solution.py:346
  69.4 1.9 %add_convert_fusion = bf16[768,2048]{1,0:T(8,128)(2,1)S(1)} fusion(f32[768,2048]{1,0:T(8,128)S(1)} %fusion.18, bf16[768,384]{1,0:T(8,128)(2,1)S(1)} %get-tuple-element.16, bf16[1,2048,384]{2,1,0:T(8,128)(2,1)S(1)} %copy-done.4), kind=kOutput, calls=%fused_computation | convolution fusion | flops 1211105280 | bytes 11599872 | tf_op jit(solution)/shard_map/dot_general | solution.py:346
  71.3 35.4 %shard_map.182 = bf16[8,96,512]{2,1,0:T(8,128)(2,1)S(1)} custom-call(bf16[8,96,2048]{2,1,0:T(8,128)(2,1)S(1)} %bitcast.89), custom_call_target="tpu_custom_call" | custom-call | tf_op jit(solution)/shard_map/pallas_call | solution.py:321
  108.0 15.6 %shard_map.183 = (bf16[4,64,2048]{2,1,0:T(8,128)(2,1)S(1)}, bf16[8,256,128]{2,1,0:T(8,128)(2,1)S(1)}) custom-call(bf16[4,64,512]{2,1,0:T(8,128)(2,1)S(1)} %bitcast.96, bf16[256,128]{1,0:T(8,128)(2,1)S(1)} %fusion.49.refs_1_), custom_call_target="tpu_custom_call" | custom-call | tf_op jit(solution)/shard_map/pallas_call | solution.py:207
  124.0 0.7 fusion.9
  125.8 1.5 collective-permute-start
  127.4 3.0 %fusion = bf16[1,2048,384]{2,1,0:T(8,128)(2,1)} fusion(bf16[768,2048]{1,0:T(8,128)(2,1)S(1)} %bitcast.101, bf16[768,384]{1,0:T(8,128)(2,1)S(1)} %get-tuple-element.17), kind=kOutput, calls=%fused_computation.8 | convolution fusion | flops 1208745984 | bytes 5308416 | tf_op jit(solution)/shard_map/dot_general | solution.py:340
  130.4 3.0 %fusion.1 = bf16[1,2048,384]{2,1,0:T(8,128)(2,1)} fusion(bf16[768,2048]{1,0:T(8,128)(2,1)S(1)} %bitcast.102, bf16[768,384]{1,0:T(8,128)(2,1)S(1)} %get-tuple-element.16), kind=kOutput, calls=%fused_computation.9 | convolution fusion | flops 1208745984 | bytes 5308416 | tf_op jit(solution)/shard_map/dot_general | solution.py:340
  133.3 2.7 %fusion.2 = bf16[1,384,2048]{2,1,0:T(8,128)(2,1)} fusion(bf16[768,2048]{1,0:T(8,128)(2,1)S(1)} %bitcast.98, f32[768,384]{1,0:T(8,128)S(1)} %fusion.14, f32[768,384]{1,0:T(8,128)S(1)} %fusion.20), kind=kOutput, calls=%fused_computation.10 | convolution fusion | flops 1211695104 | bytes 7077888 | tf_op jit(solution)/shard_map/dot_general | solution.py:340
  136.1 1.0 constant_dynamic-slice_fusion.1
  137.1 0.9 constant_dynamic-slice_fusion
  138.0 21.5 %shard_map.184 = bf16[8,4,64,256]{3,2,1,0:T(8,128)(2,1)S(1)} custom-call(bf16[8,64,256]{2,1,0:T(8,128)(2,1)S(1)} %bitcast.93, bf16[4,64,256]{2,1,0:T(8,128)(2,1)S(1)} %bitcast.95), custom_call_target="tpu_custom_call" | custom-call | tf_op jit(solution)/shard_map/pallas_call | solution.py:207
  159.5 1.1 fusion.67
  161.6 0.7 multiply_convert_fusion.3
  (62 shorter events, 5.3 us)
Async XLA Ops:
  0.6 62.7 %copy-start = (bf16[1,2048,384]{2,1,0:T(8,128)(2,1)S(1)}, bf16[1,2048,384]{2,1,0:T(8,128)(2,1)}, u32[]{:S(2)}) copy-start(bf16[1,2048,384]{2,1,0:T(8,128)(2,1)} %param.19) | copy-start | bytes 4718596
  0.6 4.0 %copy-start.1 = (bf16[256,2048]{1,0:T(8,128)(2,1)S(1)}, bf16[256,2048]{1,0:T(8,128)(2,1)}, u32[]{:S(2)}) copy-start(bf16[256,2048]{1,0:T(8,128)(2,1)} %param.15) | copy-start | bytes 3145732
  0.7 4.0 %copy-start.6 = (f32[2048]{0:T(1024)S(1)}, f32[2048]{0:T(1024)}, u32[]{:S(2)}) copy-start(f32[2048]{0:T(1024)} %param.16) | copy-start | bytes 24580
  5.9 3.0 %copy-start.2 = (bf16[256,2048]{1,0:T(8,128)(2,1)S(1)}, bf16[256,2048]{1,0:T(8,128)(2,1)}, u32[]{:S(2)}) copy-start(bf16[256,2048]{1,0:T(8,128)(2,1)} %param.14) | copy-start | bytes 3145732
  9.3 52.2 %copy-start.4 = (bf16[1,2048,384]{2,1,0:T(8,128)(2,1)S(1)}, bf16[1,2048,384]{2,1,0:T(8,128)(2,1)}, u32[]{:S(2)}) copy-start(bf16[1,2048,384]{2,1,0:T(8,128)(2,1)} %param.20) | copy-start | bytes 4718596
  63.3 1.8 %copy-start.11 = (bf16[1,384,2048]{2,1,0:T(8,128)(2,1)S(1)}, bf16[1,384,2048]{2,1,0:T(8,128)(2,1)}, u32[]{:S(2)}) copy-start(bf16[1,384,2048]{2,1,0:T(8,128)(2,1)} %param.21) | copy-start | bytes 4718596
  106.7 0.8 copy-start.5
  106.7 1.1 copy-start.10
  124.0 1.0 copy-start.12
  125.1 5.3 %copy-start.3 = (bf16[256,2048]{1,0:T(8,128)(2,1)}, bf16[256,2048]{1,0:T(8,128)(2,1)S(1)}, u32[]{:S(2)}) copy-start(bf16[256,2048]{1,0:T(8,128)(2,1)S(1)} %fusion.9) | copy-start | bytes 3145732
  125.8 34.8 %collective-permute-start = (f32[30,128]{1,0:T(8,128)S(1)}, f32[30,128]{1,0:T(8,128)S(1)}, u32[]{:S(2)}, u32[]{:S(2)}) collective-permute-start(f32[30,128]{1,0:T(8,128)S(1)} %slice.22), channel_id=1, source_target_pairs={{4,0},{8,4},{12,8},{16,12},{20,16},{24,20},{28,24},{5,1},{9,5},{13... | collective-permute-start | bytes 46088 | tf_op jit(solution)/shard_map/ppermute | solution.py:22
  138.0 22.6 %copy-start.9 = (f32[31,128]{1,0:T(8,128)S(1)}, f32[31,128]{1,0:T(8,128)}, u32[]{:S(2)}) copy-start(f32[31,128]{1,0:T(8,128)} %param.25) | copy-start | bytes 47620
  159.5 1.3 copy-start.13
  160.7 0.8 copy-start.7
  160.8 0.9 copy-start.8
where the time goes:
time: 163 us; the launch traced here: 162 us
  Pallas kernels  124 us (76%)
  matrix products  24.7 us (15%)
  other arithmetic  7.44 us (5%)
  local copies, waits for them, and re-layouts  3.37 us (2%)
    pallas_call x3, Pallas kernels, spread(): pl.pallas_call(functools.partial(spread_kernel, count, steps, over_sp, in...  89 us
    pallas_call x1, Pallas kernels, combine(): pl.pallas_call(functools.partial(combine_kernel, steps), out_shape=jax.Sh...  35.4 us
    dot_general x5, matrix products, contract_rows(): lax.dot_general(left_side, right_side, (((0,), (0,)), ((), ())), preferre...  10.2 us
    dot_general x3, matrix products, contract_cols(): lax.dot_general(left_side, right_side, (((1,), (1,)), ((), ())), preferre...  6.13 us
  transfers between devices with their start and end apart: 1, of which 0 were waited for; matrix products, arithmetic and copies ran while one was open for 7% of the time, Pallas kernels for 13%

commit v1 on v0

--- a/solution.py
+++ b/solution.py
@@ -368,6 +368,264 @@
     up_grad = contract_rows(routed_rows, up_pre_grad).astype(jnp.bfloat16)
     partial_value = contract_cols(gate_pre_grad, w_gate) + contract_cols(up_pre_grad, w_up)
     return (gate_grad, up_grad, down_grad, partial_value)
+
+
+def routed_kernel(
+    steps, send_rows, send_cots, own_rows, own_cots, w_gate, w_up, w_down,
+    gate_grad, up_grad, down_grad, out,
+    rows, cots, act, gate_pg, up_pg, part, near_in, pair, far_in, total,
+    own_sem, a_send, a_recv, b_send, f_send, c_send, near_recv, fwd_recv, far_recv,
+    n0_send, n0_recv, n1_send, n1_recv, g_send, g_recv, r_send, r_recv,
+):
+    s = lax.axis_index("sp")
+    t, near, far, diag = tp_places()
+    sends, fulls, held = (send_rows, send_cots), (own_rows, own_cots), (rows, cots)
+    width = send_rows.shape[-1]
+    hidden = w_gate.shape[1]
+    both = (0, 1)
+
+    def lanes(q):
+        return pl.ds(pl.multiple_of(q * width, width), width)
+
+    def own(c):
+        return pltpu.make_async_copy(fulls[c], held[c].at[0], own_sem.at[c])
+
+    def to_sp(c, d):
+        return pltpu.make_async_remote_copy(
+            src_ref=sends[c].at[d],
+            dst_ref=held[c].at[d, :, lanes(t)],
+            send_sem=a_send.at[c, d],
+            recv_sem=a_recv.at[c, d],
+            device_id=((s + d) % steps, t),
+            device_id_type=MESH,
+        )
+
+    def to_tp(c, d, q, target, send_sem, recv_sem):
+        return pltpu.make_async_remote_copy(
+            src_ref=held[c].at[d, :, lanes(q)],
+            dst_ref=held[c].at[d, :, lanes(q)],
+            send_sem=send_sem.at[c, d],
+            recv_sem=recv_sem.at[c, d],
+            device_id=(s, target),
+            device_id_type=MESH,
+        )
+
+    def near_copy(c, d):
+        return to_tp(c, d, t, near, b_send, near_recv)
+
+    def far_copy(c, d):
+        return to_tp(c, d, t, far, f_send, far_recv)
+
+    def fwd_copy(c, d):
+        return to_tp(c, d, far, near, c_send, fwd_recv)
+
+    def part_copy(d, which, q, send_sem, recv_sem):
+        return pltpu.make_async_remote_copy(
+            src_ref=part.at[d, :, lanes(q)],
+            dst_ref=near_in.at[which, d],
+            send_sem=send_sem.at[d],
+            recv_sem=recv_sem.at[d],
+            device_id=(s, near),
+            device_id_type=MESH,
+        )
+
+    def for_near(d):
+        return part_copy(d, 0, near, n0_send, n0_recv)
+
+    def for_diag(d):
+        return part_copy(d, 1, diag, n1_send, n1_recv)
+
+    def pair_copy(d):
+        return pltpu.make_async_remote_copy(
+            src_ref=pair.at[d],
+            dst_ref=far_in.at[d],
+            send_sem=g_send.at[d],
+            recv_sem=g_recv.at[d],
+            device_id=(s, far),
+            device_id_type=MESH,
+        )
+
+    def back(d):
+        return pltpu.make_async_remote_copy(
+            src_ref=total.at[d],
+            dst_ref=out.at[d],
+            send_sem=r_send.at[d],
+            recv_sem=r_recv.at[d],
+            device_id=((s + steps - d) % steps, t),
+            device_id_type=MESH,
+        )
+
+    def share(d):
+        for c in both:
+            to_sp(c, d).wait_recv()
+            far_copy(c, d).start()
+            near_copy(c, d).start()
+
+    def forward(d):
+        for c in both:
+            far_copy(c, d).wait_recv()
+            fwd_copy(c, d).start()
+
+    def arrived(d):
+        for c in both:
+            near_copy(c, d).wait_recv()
+            fwd_copy(c, d).wait_recv()
+
+    def experts(d):
+        gate_pre = jnp.dot(rows[d], w_gate[...], preferred_element_type=jnp.float32)
+        up_pre = jnp.dot(rows[d], w_up[...], preferred_element_type=jnp.float32)
+        act_grad = contract_cols(cots[d], w_down[...])
+        gate_clamped = jnp.minimum(gate_pre, CLAMP_LIMIT)
+        up_clamped = jnp.clip(up_pre, -CLAMP_LIMIT, CLAMP_LIMIT)
+        sigma = jax.nn.sigmoid(SLOPE_ALPHA * gate_clamped)
+        gated = gate_clamped * sigma
+        act[d] = ((up_clamped + 1.0) * gated).astype(jnp.bfloat16)
+        inside = (up_pre > -CLAMP_LIMIT) & (up_pre < CLAMP_LIMIT)
+        up_g = jnp.where(inside, act_grad * gated, 0.0).astype(jnp.bfloat16)
+        slope = sigma + SLOPE_ALPHA * gate_clamped * sigma * (1.0 - sigma)
+        gate_g = jnp.where(
+            gate_pre < CLAMP_LIMIT, act_grad * (up_clamped + 1.0) * slope, 0.0
+        ).astype(jnp.bfloat16)
+        gate_pg[d] = gate_g
+        up_pg[d] = up_g
+        for q in range(part.shape[-1] // width):
+            mine = pl.ds(q * width, width)
+            value = contract_cols(gate_g, w_gate[mine, :]) + contract_cols(up_g, w_up[mine, :])
+            part[d, :, mine] = value.astype(part.dtype)
+
+    def open_up(d):
+        for_diag(d).start()
+        for_near(d).start()
+
+    def add_pair(d):
+        for_diag(d).wait_recv()
+        mine = part[d, :, lanes(far)].astype(jnp.float32)
+        pair[d] = (mine + near_in[1, d].astype(jnp.float32)).astype(pair.dtype)
+        pair_copy(d).start()
+
+    def whole(d):
+        for_near(d).wait_recv()
+        pair_copy(d).wait_recv()
+        mine = part[d, :, lanes(t)].astype(jnp.float32)
+        summed = mine + near_in[0, d].astype(jnp.float32)
+        return (summed + far_in[d].astype(jnp.float32)).astype(out.dtype)
+
+    def flat(ref, cols):
+        return ref[:, :, cols].reshape(-1, cols.size)
+
+    every = pl.ds(0, hidden)
+
+    def row_grads(k):
+        cols = pl.ds(pl.multiple_of(k * 256, 256), 256)
+        left = flat(rows, cols)
+        gate_grad[cols, :] = contract_rows(left, flat(gate_pg, every)).astype(gate_grad.dtype)
+        up_grad[cols, :] = contract_rows(left, flat(up_pg, every)).astype(up_grad.dtype)
+
+    def act_grads(k):
+        cols = pl.ds(pl.multiple_of(k * 512, 512), 512)
+        down_grad[:, cols] = contract_rows(flat(act, every), flat(cots, cols)).astype(
+            down_grad.dtype
+        )
+
+    meet(steps, True, near, far)
+
+    def send(k):
+        for c in both:
+            to_sp(c, k).start()
+
+    looped(1, steps, send)
+    for c in both:
+        own(c).start()
+    for c in both:
+        own(c).wait()
+
+    def step(k):
+        @pl.when(k < steps)
+        def _():
+            share(k)
+
+        @pl.when((k >= 2) & (k < steps + 1))
+        def _():
+            forward(k - 1)
+
+        @pl.when(k >= 3)
+        def _():
+            arrived(k - 2)
+
+        @pl.when(k >= 2)
+        def _():
+            experts(k - 2)
+            open_up(k - 2)
+
+        @pl.when(k >= 3)
+        def _():
+            add_pair(k - 3)
+
+        @pl.when(k >= 5)
+        def _():
+            d = k - 4
+            total[d] = whole(d)
+            back(d).start()
+
+    looped(1, steps + 2, step)
+    last = steps - 1
+    half = rows.shape[-1] // 512
+    looped(0, half, row_grads)
+    add_pair(last)
+    total[last - 1] = whole(last - 1)
+    back(last - 1).start()
+    looped(half, 2 * half, row_grads)
+    total[last] = whole(last)
+    back(last).start()
+    out[0] = whole(0)
+    looped(0, half, act_grads)
+
+    def finish(d):
+        for_near(d).wait_send()
+        for_diag(d).wait_send()
+        pair_copy(d).wait_send()
+
+    def finish_remote(d):
+        for c in both:
+            to_sp(c, d).wait_send()
+            near_copy(c, d).wait_send()
+            far_copy(c, d).wait_send()
+            fwd_copy(c, d).wait_send()
+        back(d).wait()
+
+    looped(0, steps, finish)
+    looped(1, steps, finish_remote)
+
+
+def routed_experts(send_rows, send_cots, own_rows, own_cots, w_gate, w_up, w_down, collective_id):
+    steps, count, width = send_rows.shape
+    model_width, hidden = w_gate.shape
+    kind = send_rows.dtype
+    block = (steps, count, width)
+    outs = [
+        jax.ShapeDtypeStruct((model_width, hidden), kind),
+        jax.ShapeDtypeStruct((model_width, hidden), kind),
+        jax.ShapeDtypeStruct((hidden, model_width), kind),
+        jax.ShapeDtypeStruct(block, kind),
+    ]
+    pairs = pltpu.SemaphoreType.DMA((2, steps))
+    ones = pltpu.SemaphoreType.DMA((steps,))
+    return pl.pallas_call(
+        functools.partial(routed_kernel, steps),
+        out_shape=tuple(outs),
+        in_specs=[pl.BlockSpec(memory_space=pltpu.VMEM)] * 7,
+        out_specs=tuple(pl.BlockSpec(memory_space=pltpu.VMEM) for _ in outs),
+        scratch_shapes=[pltpu.VMEM((steps, count, model_width), kind)] * 2
+        + [pltpu.VMEM((steps, count, hidden), kind)] * 3
+        + [pltpu.VMEM((steps, count, model_width), kind), pltpu.VMEM((2,) + block, kind)]
+        + [pltpu.VMEM(block, kind)] * 3
+        + [pltpu.SemaphoreType.DMA((2,))]
+        + [pairs] * 8
+        + [ones] * 8,
+        compiler_params=pltpu.CompilerParams(
+            collective_id=collective_id, has_side_effects=True, vmem_limit_bytes=36 << 20
+        ),
+    )(send_rows, send_cots, own_rows, own_cots, w_gate, w_up, w_down)
 
 
 def local(
@@ -419,25 +677,38 @@
     own_rows = jnp.dot(own_pick, normed, preferred_element_type=jnp.float32).astype(jnp.bfloat16)
     own_cots = jnp.dot(own_pick, grad_out, preferred_element_type=jnp.float32)
     own_cots = (own_cots * slot_weight[:capacity]).astype(jnp.bfloat16)
-    routed_rows, routed_cots = spread(
-        (
+    if capacity % 16 == 0 and model_width % 512 == 0:
+        gate_grad, up_grad, down_grad, returned = routed_experts(
             send_rows.reshape(sp_count, capacity, col_count),
             send_cots.reshape(sp_count, capacity, col_count),
-        ),
-        (own_rows, own_cots),
-        None,
-        True,
-        False,
-        0,
-    )
-    routed_rows = routed_rows.reshape(sp_count * capacity, model_width)
-    routed_cots = routed_cots.reshape(sp_count * capacity, model_width)
-    gate_grad, up_grad, down_grad, partial_value = expert_backward(
-        routed_rows, routed_cots, gate_weight[0], up_weight[0], down_weight[0]
-    )
-    returned = combine(
-        partial_value.reshape(sp_count, capacity, model_width).astype(jnp.bfloat16), 1
-    ).reshape(sp_count * capacity, col_count)
+            own_rows,
+            own_cots,
+            gate_weight[0],
+            up_weight[0],
+            down_weight[0],
+            4,
+        )
+        returned = returned.reshape(sp_count * capacity, col_count)
+    else:
+        routed_rows, routed_cots = spread(
+            (
+                send_rows.reshape(sp_count, capacity, col_count),
+                send_cots.reshape(sp_count, capacity, col_count),
+            ),
+            (own_rows, own_cots),
+            None,
+            True,
+            False,
+            0,
+        )
+        routed_rows = routed_rows.reshape(sp_count * capacity, model_width)
+        routed_cots = routed_cots.reshape(sp_count * capacity, model_width)
+        gate_grad, up_grad, down_grad, partial_value = expert_backward(
+            routed_rows, routed_cots, gate_weight[0], up_weight[0], down_weight[0]
+        )
+        returned = combine(
+            partial_value.reshape(sp_count, capacity, model_width).astype(jnp.bfloat16), 1
+        ).reshape(sp_count * capacity, col_count)
     normed_part_grad = contract_rows(pick, returned).astype(jnp.bfloat16)
     channels = conv_sum.shape[1]
     summed = conv_sum.astype(jnp.float32).reshape(tok_rows, channels // GROUP, GROUP)

time: 163 us -> 143 us (0.88)
  matrix products: 24.7 us -> 4 us
  local copies, waits for them, and re-layouts: 3.37 us -> 10.3 us
  Pallas kernels: 124 us -> 120 us
    pallas_call x3 -> x2, Pallas kernels: 89 us -> 35.7 us  [spread(): pl.pallas_call(functools.partial(spread_kernel, count, steps, over_sp, in...]
    pallas_call x1, Pallas kernels: 35.4 us -> 84.3 us  [routed_experts(): pl.pallas_call(functools.partial(routed_kernel, steps), out_shape=tuple(o...]
    dot_general x5 -> x0, matrix products: 9.7 us -> none  [the longest x3 6.13 us: contract_cols(): lax.dot_general(left_side, right_side, (((1,), (1,)), ((), ())), preferre...]
    dot_general x5 -> x2, matrix products: 10.2 us -> 1.56 us  [contract_rows(): lax.dot_general(left_side, right_side, (((0,), (0,)), ((), ())), preferre...]
    unnamed x28 -> x39, local copies, waits for them, and re-layouts: 1.21 us -> 8.17 us
  transfers between devices with their start and end apart: 1 -> 1, of which waited for: 0 -> 0; matrix products, arithmetic and copies ran while one was open for 7% -> 2% of each run, Pallas kernels for 13% -> 15%
where the time goes in v1:
time: 143 us
  Pallas kernels  120 us (84%)
  local copies, waits for them, and re-layouts  10.3 us (7%)
  other arithmetic  6.43 us (4%)
  matrix products  4 us (3%)
    pallas_call x1, Pallas kernels, routed_experts(): pl.pallas_call(functools.partial(routed_kernel, steps), out_shape=tuple(o...  84.3 us
    pallas_call x2, Pallas kernels, spread(): pl.pallas_call(functools.partial(spread_kernel, count, steps, over_sp, in...  35.7 us
    unnamed x39, local copies, waits for them, and re-layouts  8.17 us
  transfers between devices with their start and end apart: 1, of which 0 were waited for; matrix products, arithmetic and copies ran while one was open for 2% of the time, Pallas kernels for 15%

profile of v1, /device:TPU:0, one launch (start us, length us, event | category | flops | bytes accessed | tf_op | source)
XLA Modules:
  0.0 143.1 jit_solution(14660658090268238794)
XLA Ops:
  0.7 0.8 and_select_fusion
  1.6 0.7 select_reduce_fusion.1
  3.1 1.5 %fusion.1 = f32[256]{0:T(256)S(1)} fusion(bf16[256,2048]{1,0:T(8,128)(2,1)} %param.15), kind=kLoop, calls=%fused_computation.7 | loop fusion | flops 1572608 | bytes 1049600 | tf_op jit(solution)/shard_map/reduce_sum | solution.py:653
  5.3 0.4 convolution_convert_fusion.1
  6.5 0.4 copy-done.2
  7.0 0.5 copy-done.1
  7.5 84.3 %shard_map.181 = (bf16[2048,384]{1,0:T(8,128)(2,1)S(1)}, bf16[2048,384]{1,0:T(8,128)(2,1)S(1)}, bf16[384,2048]{1,0:T(8,128)(2,1)S(1)}, bf16[8,96,512]{2,1,0:T(8,128)(2,1)S(1)}) custom-call(bf16[8,96,512]{2,1,0:T(8,128)(2,1)S(1)} %bitcast.62, bf16[8,96,512]{2,1,0:T(8,128)(2,1)S(1)} %bitcast.63, bf16[96,2048]{1,0:T(8,128)(2,1)S(1)} %convolution_convert_fusion.own_rows, ...), custom_call_target="tpu_custom_call" | custom-call | tf_op jit(solution)/shard_map/pallas_call | solution.py:613
  91.8 0.4 fusion.10
  92.3 0.5 copy-done.11
  93.2 14.2 %shard_map.182 = (bf16[4,64,2048]{2,1,0:T(8,128)(2,1)S(1)}, bf16[8,256,128]{2,1,0:T(8,128)(2,1)S(1)}) custom-call(bf16[4,64,512]{2,1,0:T(8,128)(2,1)S(1)} %bitcast.73, bf16[256,128]{1,0:T(8,128)(2,1)S(1)} %fusion.34.refs_1_), custom_call_target="tpu_custom_call" | custom-call | tf_op jit(solution)/shard_map/pallas_call | solution.py:207
  107.5 0.4 fusion.7
  107.9 0.7 fusion.6
  108.7 1.0 copy-done.10
  109.6 0.5 fusion.48
  110.4 1.3 collective-permute-start
  111.7 1.0 constant_dynamic-slice_fusion.1
  112.7 0.9 constant_dynamic-slice_fusion
  113.7 21.5 %shard_map.183 = bf16[8,4,64,256]{3,2,1,0:T(8,128)(2,1)S(1)} custom-call(bf16[8,64,256]{2,1,0:T(8,128)(2,1)S(1)} %bitcast.70, bf16[4,64,256]{2,1,0:T(8,128)(2,1)S(1)} %bitcast.72), custom_call_target="tpu_custom_call" | custom-call | tf_op jit(solution)/shard_map/pallas_call | solution.py:207
  135.1 1.1 fusion.49
  136.8 0.4 copy-done.13
  137.3 0.7 multiply_convert_fusion.1
  138.0 2.8 %copy.50 = bf16[1,2048,384]{2,1,0:T(8,128)(2,1)} copy(bf16[1,2048,384]{2,1,0:T(8,128)(2,1)} %bitcast.69) | data formatting | bytes 3145728
  140.8 1.1 copy.51
  142.0 1.1 copy.52
  (64 shorter events, 3.6 us)
Async XLA Ops:
  0.6 109.0 %copy-start = (bf16[2048,128]{1,0:T(8,128)(2,1)S(1)}, bf16[2048,128]{1,0:T(8,128)(2,1)}, u32[]{:S(2)}) copy-start(bf16[2048,128]{1,0:T(8,128)(2,1)} %param.22) | copy-start | bytes 1572868
  0.6 3.9 %copy-start.7 = (bf16[256,2048]{1,0:T(8,128)(2,1)S(1)}, bf16[256,2048]{1,0:T(8,128)(2,1)}, u32[]{:S(2)}) copy-start(bf16[256,2048]{1,0:T(8,128)(2,1)} %param.15) | copy-start | bytes 3145732
  0.7 3.9 %copy-start.12 = (f32[2048]{0:T(1024)S(1)}, f32[2048]{0:T(1024)}, u32[]{:S(2)}) copy-start(f32[2048]{0:T(1024)} %param.16) | copy-start | bytes 24580
  4.6 1.2 copy-start.9
  4.9 1.6 %copy-start.3 = (bf16[1,384,2048]{2,1,0:T(8,128)(2,1)S(1)}, bf16[1,384,2048]{2,1,0:T(8,128)(2,1)}, u32[]{:S(2)}) copy-start(bf16[1,384,2048]{2,1,0:T(8,128)(2,1)} %param.21) | copy-start | bytes 4718596
  5.3 1.7 %copy-start.2 = (bf16[1,2048,384]{2,1,0:T(8,128)(2,1)S(1)}, bf16[1,2048,384]{2,1,0:T(8,128)(2,1)}, u32[]{:S(2)}) copy-start(bf16[1,2048,384]{2,1,0:T(8,128)(2,1)} %param.20) | copy-start | bytes 4718596
  5.8 1.6 %copy-start.1 = (bf16[1,2048,384]{2,1,0:T(8,128)(2,1)S(1)}, bf16[1,2048,384]{2,1,0:T(8,128)(2,1)}, u32[]{:S(2)}) copy-start(bf16[1,2048,384]{2,1,0:T(8,128)(2,1)} %param.19) | copy-start | bytes 4718596
  91.8 16.1 %copy-start.4 = (bf16[2048,384]{1,0:T(8,128)(2,1)}, bf16[2048,384]{1,0:T(8,128)(2,1)S(1)}, u32[]{:S(2)}) copy-start(bf16[2048,384]{1,0:T(8,128)(2,1)S(1)} %get-tuple-element.13) | copy-start | bytes 4718596
  91.8 16.1 %copy-start.6 = (bf16[2048,384]{1,0:T(8,128)(2,1)}, bf16[2048,384]{1,0:T(8,128)(2,1)S(1)}, u32[]{:S(2)}) copy-start(bf16[2048,384]{1,0:T(8,128)(2,1)S(1)} %get-tuple-element.12) | copy-start | bytes 4718596
  91.8 0.9 copy-start.11
  91.8 1.2 copy-start.16
  91.8 15.6 %copy-start.8 = (bf16[256,2048]{1,0:T(8,128)(2,1)S(1)}, bf16[256,2048]{1,0:T(8,128)(2,1)}, u32[]{:S(2)}) copy-start(bf16[256,2048]{1,0:T(8,128)(2,1)} %param.15) | copy-start | bytes 3145732
  108.7 1.0 copy-start.10
  110.4 25.9 %collective-permute-start = (f32[30,128]{1,0:T(8,128)S(1)}, f32[30,128]{1,0:T(8,128)S(1)}, u32[]{:S(2)}, u32[]{:S(2)}) collective-permute-start(f32[30,128]{1,0:T(8,128)S(1)} %slice.22), channel_id=1, source_target_pairs={{4,0},{8,4},{12,8},{16,12},{20,16},{24,20},{28,24},{5,1},{9,5},{13... | collective-permute-start | bytes 46088 | tf_op jit(solution)/shard_map/ppermute | solution.py:22
  113.6 22.6 %copy-start.15 = (f32[31,128]{1,0:T(8,128)S(1)}, f32[31,128]{1,0:T(8,128)}, u32[]{:S(2)}) copy-start(f32[31,128]{1,0:T(8,128)} %param.25) | copy-start | bytes 47620
  135.1 1.3 copy-start.17
  136.4 0.8 copy-start.13
  136.4 0.9 copy-start.14
  138.0 2.8 %copy-start.5 = (bf16[2048,384]{1,0:T(8,128)(2,1)S(1)}, bf16[2048,384]{1,0:T(8,128)(2,1)}, u32[]{:S(2)}) copy-start(bf16[2048,384]{1,0:T(8,128)(2,1)} %copy-done.4) | copy-start | bytes 4718596

commit v2 on v1

--- a/solution.py
+++ b/solution.py
@@ -371,11 +371,11 @@
 
 
 def routed_kernel(
-    steps, send_rows, send_cots, own_rows, own_cots, w_gate, w_up, w_down,
-    gate_grad, up_grad, down_grad, out,
+    steps, send_rows, send_cots, own_rows, own_cots, w_gate, w_up, w_down, side,
+    gate_grad, up_grad, down_grad, out, side_out,
     rows, cots, act, gate_pg, up_pg, part, near_in, pair, far_in, total,
     own_sem, a_send, a_recv, b_send, f_send, c_send, near_recv, fwd_recv, far_recv,
-    n0_send, n0_recv, n1_send, n1_recv, g_send, g_recv, r_send, r_recv,
+    n0_send, n0_recv, n1_send, n1_recv, g_send, g_recv, r_send, r_recv, s_send, s_recv,
 ):
     s = lax.axis_index("sp")
     t, near, far, diag = tp_places()
@@ -452,6 +452,19 @@
             send_sem=r_send.at[d],
             recv_sem=r_recv.at[d],
             device_id=((s + steps - d) % steps, t),
+            device_id_type=MESH,
+        )
+
+    def own_side():
+        return pltpu.make_async_copy(side, side_out.at[0], own_sem.at[2])
+
+    def side_copy(d):
+        return pltpu.make_async_remote_copy(
+            src_ref=side,
+            dst_ref=side_out.at[d],
+            send_sem=s_send.at[d],
+            recv_sem=s_recv.at[d],
+            device_id=((s + d) % steps, t),
             device_id_type=MESH,
         )
 
@@ -534,6 +547,7 @@
             to_sp(c, k).start()
 
     looped(1, steps, send)
+    own_side().start()
     for c in both:
         own(c).start()
     for c in both:
@@ -543,6 +557,7 @@
         @pl.when(k < steps)
         def _():
             share(k)
+            side_copy(k).start()
 
         @pl.when((k >= 2) & (k < steps + 1))
         def _():
@@ -592,12 +607,16 @@
             far_copy(c, d).wait_send()
             fwd_copy(c, d).wait_send()
         back(d).wait()
-
+        side_copy(d).wait()
+
+    own_side().wait()
     looped(0, steps, finish)
     looped(1, steps, finish_remote)
 
 
-def routed_experts(send_rows, send_cots, own_rows, own_cots, w_gate, w_up, w_down, collective_id):
+def routed_experts(
+    send_rows, send_cots, own_rows, own_cots, w_gate, w_up, w_down, side, collective_id
+):
     steps, count, width = send_rows.shape
     model_width, hidden = w_gate.shape
     kind = send_rows.dtype
@@ -607,25 +626,285 @@
         jax.ShapeDtypeStruct((model_width, hidden), kind),
         jax.ShapeDtypeStruct((hidden, model_width), kind),
         jax.ShapeDtypeStruct(block, kind),
+        jax.ShapeDtypeStruct((steps,) + side.shape, side.dtype),
     ]
     pairs = pltpu.SemaphoreType.DMA((2, steps))
     ones = pltpu.SemaphoreType.DMA((steps,))
     return pl.pallas_call(
         functools.partial(routed_kernel, steps),
         out_shape=tuple(outs),
-        in_specs=[pl.BlockSpec(memory_space=pltpu.VMEM)] * 7,
+        in_specs=[pl.BlockSpec(memory_space=pltpu.VMEM)] * 8,
         out_specs=tuple(pl.BlockSpec(memory_space=pltpu.VMEM) for _ in outs),
         scratch_shapes=[pltpu.VMEM((steps, count, model_width), kind)] * 2
         + [pltpu.VMEM((steps, count, hidden), kind)] * 3
         + [pltpu.VMEM((steps, count, model_width), kind), pltpu.VMEM((2,) + block, kind)]
         + [pltpu.VMEM(block, kind)] * 3
-        + [pltpu.SemaphoreType.DMA((2,))]
+        + [pltpu.SemaphoreType.DMA((3,))]
         + [pairs] * 8
-        + [ones] * 8,
+        + [ones] * 10,
         compiler_params=pltpu.CompilerParams(
             collective_id=collective_id, has_side_effects=True, vmem_limit_bytes=36 << 20
         ),
-    )(send_rows, send_cots, own_rows, own_cots, w_gate, w_up, w_down)
+    )(send_rows, send_cots, own_rows, own_cots, w_gate, w_up, w_down, side)
+
+
+def settle_kernel(
+    steps, part_grad, grad_out, resid, inv_rms, norm_gain, proj_weight,
+    conv_sum, conv_gain, conv_taps, conv_value, conv_gate,
+    feature_cols, value_grad, gate_input_grad,
+    full, grads, extended, far_send, far_recv, near_send, near_recv, fwd_send, fwd_recv,
+    own_sem, x_send, x_recv, xf_send, xf_recv, xn_send, xn_recv, xw_send, xw_recv,
+    h_send, h_recv,
+):
+    s = lax.axis_index("sp")
+    t, near, far, diag = tp_places()
+    tok_rows, width = part_grad.shape
+    chunks, share = feature_cols.shape[1], feature_cols.shape[2]
+    feat_rows = feature_cols.shape[3]
+    overlap = conv_taps.shape[0] - 1
+
+    def rows_of(j):
+        return pl.ds(pl.multiple_of(j * share, share), share)
+
+    def lanes(q):
+        return pl.ds(pl.multiple_of(q * width, width), width)
+
+    def mine_at(j):
+        return full.at[rows_of(j), lanes(t)]
+
+    def own_copy():
+        return pltpu.make_async_copy(part_grad, full.at[:, lanes(t)], own_sem.at[0])
+
+    def gather(j, q, src, target, send_sem, recv_sem):
+        return pltpu.make_async_remote_copy(
+            src_ref=src,
+            dst_ref=full.at[rows_of(j), lanes(q)],
+            send_sem=send_sem.at[j],
+            recv_sem=recv_sem.at[j],
+            device_id=(s, target),
+            device_id_type=MESH,
+        )
+
+    def to_far(j):
+        return gather(j, t, part_grad.at[rows_of(j), :], far, far_send, far_recv)
+
+    def to_near(j):
+        return gather(j, t, part_grad.at[rows_of(j), :], near, near_send, near_recv)
+
+    def pass_near(j):
+        return gather(j, far, full.at[rows_of(j), lanes(far)], near, fwd_send, fwd_recv)
+
+    def spread_out(d):
+        feats = pl.ds(pl.multiple_of(((s + d) % steps) * feat_rows, feat_rows), feat_rows)
+        return pltpu.make_async_remote_copy(
+            src_ref=grads.at[rows_of(t), feats],
+            dst_ref=feature_cols.at[d, t],
+            send_sem=x_send.at[d],
+            recv_sem=x_recv.at[d],
+            device_id=((s + d) % steps, t),
+            device_id_type=MESH,
+        )
+
+    def beside(d, q, target, send_sem, recv_sem):
+        return pltpu.make_async_remote_copy(
+            src_ref=feature_cols.at[d, q],
+            dst_ref=feature_cols.at[d, q],
+            send_sem=send_sem.at[d],
+            recv_sem=recv_sem.at[d],
+            device_id=(s, target),
+            device_id_type=MESH,
+        )
+
+    def x_far(d):
+        return beside(d, t, far, xf_send, xf_recv)
+
+    def x_near(d):
+        return beside(d, t, near, xn_send, xn_recv)
+
+    def x_pass(d):
+        return beside(d, far, near, xw_send, xw_recv)
+
+    def halo():
+        return pltpu.make_async_remote_copy(
+            src_ref=extended.at[pl.ds(0, overlap + 2)],
+            dst_ref=extended.at[pl.ds(tok_rows, overlap + 2)],
+            send_sem=h_send.at[0],
+            recv_sem=h_recv.at[0],
+            device_id=((s + steps - 1) % steps, t),
+            device_id_type=MESH,
+        )
+
+    gain = norm_gain[...]
+
+    def settle(j):
+        here = rows_of(j)
+        feature_grad = full[here, :].astype(jnp.float32) * gain
+        x = resid[here, :].astype(jnp.float32)
+        scale = inv_rms[here, :]
+        cubed = scale * scale * scale
+        mean = jnp.mean(x * feature_grad, axis=-1, keepdims=True)
+        value = grad_out[here, :].astype(jnp.float32) + scale * feature_grad - x * cubed * mean
+        grads[here, :] = value.astype(grads.dtype)
+
+    def crossing(k):
+        return crossing_first(steps, k)
+
+    meet(steps, True, near, far)
+    for j in (far, diag, t, near):
+        to_far(j).start()
+    for j in (near, t, diag, far):
+        to_near(j).start()
+    own_copy().start()
+    summed = conv_sum[...].astype(jnp.float32)
+    centre = summed - jnp.mean(summed, axis=-1, keepdims=True)
+    inv_std = lax.rsqrt(jnp.mean(centre * centre, axis=-1, keepdims=True) + 1e-05)
+    grouped = centre * inv_std
+    pre_act = grouped * conv_gain[...]
+    sigma = jax.nn.sigmoid(pre_act)
+    slope = sigma * (1.0 + pre_act * (1.0 - sigma)) * conv_gain[...]
+    own_copy().wait()
+
+    def arrive(j):
+        to_far(j).wait_recv()
+        pass_near(j).start()
+
+    def whole(j):
+        to_near(j).wait_recv()
+        pass_near(j).wait_recv()
+
+    arrive(t)
+    arrive(near)
+    whole(t)
+    settle(t)
+    looped(0, steps - 1, lambda k: spread_out(crossing(k)).start())
+    arrive(far)
+    arrive(diag)
+    for j in (near, far, diag):
+        whole(j)
+        settle(j)
+    feats = pl.ds(pl.multiple_of(s * feat_rows, feat_rows), feat_rows)
+    feature_cols[0] = grads[:, feats].reshape(chunks, share, feat_rows)
+    out_grad = jnp.dot(grads[...], proj_weight[...], preferred_element_type=jnp.float32)
+    normal = out_grad * slope
+    sum_grad = inv_std * (
+        normal
+        - jnp.mean(normal, axis=-1, keepdims=True)
+        - grouped * jnp.mean(normal * grouped, axis=-1, keepdims=True)
+    )
+    extended[pl.ds(0, tok_rows), :] = sum_grad
+    halo().start()
+
+    def share_out(d):
+        spread_out(d).wait_recv()
+        x_far(d).start()
+        x_near(d).start()
+
+    def pass_on(d):
+        x_far(d).wait_recv()
+        x_pass(d).start()
+
+    def both(k):
+        share_out(crossing(k))
+        pass_on(crossing(k - 1))
+
+    share_out(crossing(0))
+    looped(1, steps - 1, both)
+    halo().wait()
+
+    @pl.when(s == steps - 1)
+    def _():
+        extended[pl.ds(tok_rows, overlap + 2), :] = jnp.zeros(
+            (overlap + 2, extended.shape[1]), extended.dtype
+        )
+
+    gated_grad = extended[pl.ds(overlap, tok_rows), :] * conv_taps[pl.ds(0, 1), :]
+    for j in range(1, overlap + 1):
+        gated_grad += extended[pl.ds(overlap - j, tok_rows), :] * conv_taps[pl.ds(j, 1), :]
+    sigma_gate = jax.nn.sigmoid(conv_gate[...].astype(jnp.float32))
+    value_grad[...] = (gated_grad * sigma_gate).astype(value_grad.dtype)
+    gate_input_grad[...] = (
+        gated_grad * conv_value[...].astype(jnp.float32) * sigma_gate * (1.0 - sigma_gate)
+    ).astype(gate_input_grad.dtype)
+    pass_on(crossing(steps - 2))
+
+    def finish(k):
+        d = crossing(k)
+        spread_out(d).wait_send()
+        x_near(d).wait()
+        x_far(d).wait_send()
+        x_pass(d).wait()
+
+    looped(0, steps - 1, finish)
+
+    def finish_gather(j):
+        to_far(j).wait_send()
+        to_near(j).wait_send()
+        pass_near(j).wait_send()
+
+    looped(0, chunks, finish_gather)
+
+
+def settle_tokens(operands, collective_id):
+    part_grad, resid, conv_sum = operands[0], operands[2], operands[6]
+    overlap = operands[8].shape[0] - 1
+    steps, tp_count = lax.axis_size("sp"), lax.axis_size("tp")
+    tok_rows, model_width = resid.shape
+    channels = conv_sum.shape[1]
+    kind = resid.dtype
+    outs = [
+        jax.ShapeDtypeStruct((steps, tp_count, tok_rows // tp_count, model_width // steps), kind),
+        jax.ShapeDtypeStruct((tok_rows, channels), kind),
+        jax.ShapeDtypeStruct((tok_rows, channels), kind),
+    ]
+    fours = pltpu.SemaphoreType.DMA((tp_count,))
+    ones = pltpu.SemaphoreType.DMA((steps,))
+    single = pltpu.SemaphoreType.DMA((1,))
+    return pl.pallas_call(
+        functools.partial(settle_kernel, steps),
+        out_shape=tuple(outs),
+        in_specs=[pl.BlockSpec(memory_space=pltpu.VMEM)] * len(operands),
+        out_specs=tuple(pl.BlockSpec(memory_space=pltpu.VMEM) for _ in outs),
+        scratch_shapes=[
+            pltpu.VMEM((tok_rows, model_width), kind),
+            pltpu.VMEM((tok_rows, model_width), kind),
+            pltpu.VMEM((tok_rows + overlap + 2, channels), jnp.float32),
+        ]
+        + [fours] * 6
+        + [single]
+        + [ones] * 8
+        + [single] * 2,
+        compiler_params=pltpu.CompilerParams(
+            collective_id=collective_id, has_side_effects=True, vmem_limit_bytes=24 << 20
+        ),
+    )(*operands)
+
+
+def last_kernel(feature_cols, all_out, gate_in, up_in, down_in, proj, gate_out, up_out, down_out, sem):
+    moves = [
+        pltpu.make_async_copy(a, b, sem.at[i])
+        for i, (a, b) in enumerate(((gate_in, gate_out), (up_in, up_out), (down_in, down_out)))
+    ]
+    for move in moves:
+        move.start()
+    proj[...] = contract_rows(feature_cols[...], all_out[...])
+    for move in moves:
+        move.wait()
+
+
+def last_stage(feature_cols, all_out, grads):
+    held = [pl.BlockSpec(memory_space=pltpu.VMEM)]
+    outside = [pl.BlockSpec(memory_space=pl.ANY)]
+    shape = (feature_cols.shape[1], all_out.shape[1])
+    outs = [jax.ShapeDtypeStruct(shape, jnp.float32)]
+    outs += [jax.ShapeDtypeStruct(g.shape, g.dtype) for g in grads]
+    return pl.pallas_call(
+        last_kernel,
+        out_shape=tuple(outs),
+        in_specs=held * 5,
+        out_specs=tuple(held + outside * 3),
+        scratch_shapes=[pltpu.SemaphoreType.DMA((3,))],
+        compiler_params=pltpu.CompilerParams(vmem_limit_bytes=16 << 20),
+    )(feature_cols, all_out, *grads)
 
 
 def local(
@@ -677,8 +956,18 @@
     own_rows = jnp.dot(own_pick, normed, preferred_element_type=jnp.float32).astype(jnp.bfloat16)
     own_cots = jnp.dot(own_pick, grad_out, preferred_element_type=jnp.float32)
     own_cots = (own_cots * slot_weight[:capacity]).astype(jnp.bfloat16)
-    if capacity % 16 == 0 and model_width % 512 == 0:
-        gate_grad, up_grad, down_grad, returned = routed_experts(
+    channels = conv_sum.shape[1]
+    summed = conv_sum.astype(jnp.float32).reshape(tok_rows, channels // GROUP, GROUP)
+    centre = summed - jnp.mean(summed, axis=-1, keepdims=True)
+    inv_std = lax.rsqrt(jnp.mean(centre * centre, axis=-1, keepdims=True) + 1e-05)
+    grouped = centre * inv_std
+    chan_normed = grouped.reshape(tok_rows, channels)
+    pre_act = chan_normed * conv_gain
+    sigma_conv = jax.nn.sigmoid(pre_act)
+    conv_out = (pre_act * sigma_conv).astype(jnp.bfloat16)
+    aligned = capacity % 16 == 0 and model_width % (128 * sp_count) == 0 and channels == GROUP
+    if aligned:
+        gate_grad, up_grad, down_grad, returned, all_out = routed_experts(
             send_rows.reshape(sp_count, capacity, col_count),
             send_cots.reshape(sp_count, capacity, col_count),
             own_rows,
@@ -686,6 +975,7 @@
             gate_weight[0],
             up_weight[0],
             down_weight[0],
+            conv_out,
             4,
         )
         returned = returned.reshape(sp_count * capacity, col_count)
@@ -710,15 +1000,29 @@
             partial_value.reshape(sp_count, capacity, model_width).astype(jnp.bfloat16), 1
         ).reshape(sp_count * capacity, col_count)
     normed_part_grad = contract_rows(pick, returned).astype(jnp.bfloat16)
-    channels = conv_sum.shape[1]
-    summed = conv_sum.astype(jnp.float32).reshape(tok_rows, channels // GROUP, GROUP)
-    centre = summed - jnp.mean(summed, axis=-1, keepdims=True)
-    inv_std = lax.rsqrt(jnp.mean(centre * centre, axis=-1, keepdims=True) + 1e-05)
-    grouped = centre * inv_std
-    chan_normed = grouped.reshape(tok_rows, channels)
-    pre_act = chan_normed * conv_gain
-    sigma_conv = jax.nn.sigmoid(pre_act)
-    conv_out = (pre_act * sigma_conv).astype(jnp.bfloat16)
+    if aligned:
+        operands = (
+            normed_part_grad,
+            grad_out,
+            resid,
+            inv_rms,
+            norm_gain[None],
+            proj_weight,
+            conv_sum,
+            conv_gain[None],
+            conv_taps,
+            conv_value,
+            conv_gate,
+        )
+        feature_cols, value_grad, gate_input_grad = settle_tokens(operands, 5)
+        feat_rows = model_width // sp_count
+        proj_grad, gate_grad, up_grad, down_grad = last_stage(
+            feature_cols.reshape(sp_count * tok_rows, feat_rows),
+            all_out.reshape(sp_count * tok_rows, channels),
+            (gate_grad, up_grad, down_grad),
+        )
+        weight_grads = (gate_grad[None], up_grad[None], down_grad[None])
+        return weight_grads + (proj_grad, value_grad, gate_input_grad)
     chunks = 4
     normed_grad, all_out = spread(
         (normed_part_grad.reshape(chunks, tok_rows // chunks, col_count),),

time: 143 us -> 131 us (0.916)
  local copies, waits for them, and re-layouts: 10.3 us -> 3.77 us
  matrix products: 4 us -> 1.98 us
  Pallas kernels: 120 us -> 118 us
    pallas_call x2, Pallas kernels: 35.7 us -> 26.1 us  [the longest x1 23 us: settle_tokens(): pl.pallas_call(functools.partial(settle_kernel, steps), out_shape=tuple(o...]
    pallas_call x1, Pallas kernels: 84.3 us -> 91.5 us  [routed_experts(): pl.pallas_call(functools.partial(routed_kernel, steps), out_shape=tuple(o...]
    unnamed x39 -> x26, local copies, waits for them, and re-layouts: 8.17 us -> 3.48 us
    dynamic_slice x2 -> x0, local copies, waits for them, and re-layouts: 1.89 us -> none  [the longest x1 0.97 us: local(): lax.dynamic_slice_in_dim(resid_grad, lax.axis_index('tp') * share, share, 0)]
    convert_element_type x2 -> x0, other arithmetic: 1.45 us -> none  [the longest x1 0.73 us: local(): resid_grad = (grad_out.astype(jnp.float32) + inv_rms * feature_grad - res...]
  transfers between devices with their start and end apart: 1 -> 0, of which waited for: 0 -> 0; matrix products, arithmetic and copies ran while one was open for 2% -> 0% of each run, Pallas kernels for 15% -> 0%
where the time goes in v2:
time: 131 us
  Pallas kernels  118 us (90%)
  other arithmetic  6.81 us (5%)
  local copies, waits for them, and re-layouts  3.77 us (3%)
  matrix products  1.98 us (2%)
    pallas_call x1, Pallas kernels, routed_experts(): pl.pallas_call(functools.partial(routed_kernel, steps), out_shape=tuple(o...  91.5 us
    pallas_call x1, Pallas kernels, settle_tokens(): pl.pallas_call(functools.partial(settle_kernel, steps), out_shape=tuple(o...  23 us
    unnamed x26, local copies, waits for them, and re-layouts  3.48 us
    pallas_call x1, Pallas kernels, last_stage(): pl.pallas_call(last_kernel, out_shape=tuple(outs), in_specs=held * 5, out...  3.03 us

profile of v2, /device:TPU:0, one launch (start us, length us, event | category | flops | bytes accessed | tf_op | source)
XLA Modules:
  0.0 131.0 jit_solution(15060894222459836589)
XLA Ops:
  0.6 1.6 %fusion.1 = f32[256]{0:T(256)S(1)} fusion(bf16[256,2048]{1,0:T(8,128)(2,1)} %resid.1), kind=kLoop, calls=%fused_computation.5 | loop fusion | flops 1572608 | bytes 1049600 | tf_op jit(solution)/shard_map/reduce_sum | solution.py:932
  2.3 0.9 convert_reduce_fusion
  3.2 1.0 fusion.11
  4.3 0.7 and_select_fusion
  5.2 0.7 select_reduce_fusion.1
  5.9 0.2 select_reduce_fusion
  6.2 1.0 fusion.18.side
  7.7 0.3 fusion.own_cots
  8.0 0.4 multiply_convert_fusion
  8.4 0.2 copy-done
  8.6 0.3 fusion.3
  8.9 0.3 convolution_convert_fusion.own_rows
  9.3 0.4 convolution_convert_fusion.1
  9.6 0.4 copy-done.3
  10.0 0.5 copy-done.4
  10.5 0.6 copy-done.2
  11.0 91.5 %shard_map.181 = (bf16[2048,384]{1,0:T(8,128)(2,1)S(1)}, bf16[2048,384]{1,0:T(8,128)(2,1)S(1)}, bf16[384,2048]{1,0:T(8,128)(2,1)S(1)}, bf16[8,96,512]{2,1,0:T(8,128)(2,1)S(1)}, bf16[8,256,128]{2,1,0:T(8,128)(2,1)S(1)}) custom-call(bf16[8,96,512]{2,1,0:T(8,128)(2,1)S(1)} %bitcast.35, bf16[8,96,512]{2,1,0:T(8,128)(2,1)S(1)} %bitcast.34, ...), custom_call_target="tpu_custom_call" | custom-call | tf_op jit(solution)/shard_map/pallas_call | solution.py:633
  102.6 0.4 fusion.4.part_grad
  103.0 0.3 copy-done.5
  103.4 0.2 copy-done.6
  103.6 23.0 %shard_map.182 = (bf16[8,4,64,256]{3,2,1,0:T(8,128)(2,1)S(1)}, bf16[256,128]{1,0:T(8,128)(2,1)S(1)}, bf16[256,128]{1,0:T(8,128)(2,1)S(1)}) custom-call(bf16[256,512]{1,0:T(8,128)(2,1)S(1)} %fusion.4.part_grad, bf16[256,2048]{1,0:T(8,128)(2,1)S(1)} %copy-done.1, bf16[256,2048]{1,0:T(8,128)(2,1)S(1)} %copy-done, f32[256,1]{1,0:T(8,128)S(1)} %copy.25.inv_rms, ...), custom_call_target="tpu_custom_call" | custom-call | tf_op jit(solution)/shard_map/pallas_call | solution.py:862
  126.7 3.0 %shard_map.183 = (f32[256,128]{1,0:T(8,128)}, bf16[2048,384]{1,0:T(8,128)(2,1)}, bf16[2048,384]{1,0:T(8,128)(2,1)}, bf16[384,2048]{1,0:T(8,128)(2,1)}) custom-call(bf16[2048,256]{1,0:T(8,128)(2,1)S(1)} %bitcast.39, bf16[2048,128]{1,0:T(8,128)(2,1)S(1)} %bitcast.40, bf16[2048,384]{1,0:T(8,128)(2,1)S(1)} %get-tuple-element.21.gate_in, ...), custom_call_target="tpu_custom_call" | custom-call | tf_op jit(solution)/shard_map/pallas_call | solution.py:900
  129.7 0.6 copy.32
  130.3 0.6 copy.33
  (30 shorter events, 0.8 us)
Async XLA Ops:
  0.6 7.1 %copy-start.1 = (bf16[256,2048]{1,0:T(8,128)(2,1)S(1)}, bf16[256,2048]{1,0:T(8,128)(2,1)}, u32[]{:S(2)}) copy-start(bf16[256,2048]{1,0:T(8,128)(2,1)} %grad_out.1) | copy-start | bytes 3145732
  7.4 1.2 copy-start
  7.4 1.2 copy-start.9
  8.6 1.4 %copy-start.3 = (bf16[1,2048,384]{2,1,0:T(8,128)(2,1)S(1)}, bf16[1,2048,384]{2,1,0:T(8,128)(2,1)}, u32[]{:S(2)}) copy-start(bf16[1,2048,384]{2,1,0:T(8,128)(2,1)} %param.20) | copy-start | bytes 4718596
  8.6 1.9 %copy-start.4 = (bf16[1,384,2048]{2,1,0:T(8,128)(2,1)S(1)}, bf16[1,384,2048]{2,1,0:T(8,128)(2,1)}, u32[]{:S(2)}) copy-start(bf16[1,384,2048]{2,1,0:T(8,128)(2,1)} %param.21) | copy-start | bytes 4718596
  8.9 2.1 %copy-start.2 = (bf16[1,2048,384]{2,1,0:T(8,128)(2,1)S(1)}, bf16[1,2048,384]{2,1,0:T(8,128)(2,1)}, u32[]{:S(2)}) copy-start(bf16[1,2048,384]{2,1,0:T(8,128)(2,1)} %param.19) | copy-start | bytes 4718596
  102.5 0.8 copy-start.5
  102.5 1.1 copy-start.6
  102.5 1.1 copy-start.7
  102.6 1.1 copy-start.8
  102.6 1.0 copy-start.10
  102.6 1.0 copy-start.11

commit v3 on v2

--- a/solution.py
+++ b/solution.py
@@ -370,286 +370,530 @@
     return (gate_grad, up_grad, down_grad, partial_value)
 
 
-def routed_kernel(
-    steps, send_rows, send_cots, own_rows, own_cots, w_gate, w_up, w_down, side,
-    gate_grad, up_grad, down_grad, out, side_out,
-    rows, cots, act, gate_pg, up_pg, part, near_in, pair, far_in, total,
-    own_sem, a_send, a_recv, b_send, f_send, c_send, near_recv, fwd_recv, far_recv,
+def relay_kernel(
+    steps, info, grad_out, resid, norm_gain, gate_held, up_held, down_held, conv_sum, conv_gain,
+    gate_grad, up_grad, down_grad, part_grad, side_out,
+    w_gate, w_up, w_down, normed, infos, ranks, weights, before, picks,
+    tok, over, cross, cross_far, held, act, gate_pg, up_pg, part,
+    near_in, pair, far_in, total, ret, side,
+    own_sem, info_send, info_recv, line_send, line_recv, end_send, cross_recv,
+    across_send, afar_send, arr_recv, b_send, f_send, c_send, near_recv, fwd_recv, far_recv,
     n0_send, n0_recv, n1_send, n1_recv, g_send, g_recv, r_send, r_recv, s_send, s_recv,
 ):
     s = lax.axis_index("sp")
     t, near, far, diag = tp_places()
-    sends, fulls, held = (send_rows, send_cots), (own_rows, own_cots), (rows, cots)
-    width = send_rows.shape[-1]
+    line = steps // 2
+    z, y = s // 2, s % 2
+    across = s + 1 - 2 * y
+    tok_rows, width = part_grad.shape
+    count = cross.shape[2]
     hidden = w_gate.shape[1]
+    model_width = resid.shape[1]
     both = (0, 1)
+    kind = held.dtype
+    sources = (grad_out, normed)
 
     def lanes(q):
         return pl.ds(pl.multiple_of(q * width, width), width)
 
-    def own(c):
-        return pltpu.make_async_copy(fulls[c], held[c].at[0], own_sem.at[c])
-
-    def to_sp(c, d):
+    def remote(src, dst, send_sem, recv_sem, sp_to, tp_to):
         return pltpu.make_async_remote_copy(
-            src_ref=sends[c].at[d],
-            dst_ref=held[c].at[d, :, lanes(t)],
-            send_sem=a_send.at[c, d],
-            recv_sem=a_recv.at[c, d],
-            device_id=((s + d) % steps, t),
+            src_ref=src,
+            dst_ref=dst,
+            send_sem=send_sem,
+            recv_sem=recv_sem,
+            device_id=(sp_to, tp_to),
             device_id_type=MESH,
         )
 
-    def to_tp(c, d, q, target, send_sem, recv_sem):
-        return pltpu.make_async_remote_copy(
-            src_ref=held[c].at[d, :, lanes(q)],
-            dst_ref=held[c].at[d, :, lanes(q)],
-            send_sem=send_sem.at[c, d],
-            recv_sem=recv_sem.at[c, d],
-            device_id=(s, target),
-            device_id_type=MESH,
-        )
-
-    def near_copy(c, d):
-        return to_tp(c, d, t, near, b_send, near_recv)
-
-    def far_copy(c, d):
-        return to_tp(c, d, t, far, f_send, far_recv)
-
-    def fwd_copy(c, d):
-        return to_tp(c, d, far, near, c_send, fwd_recv)
-
-    def part_copy(d, which, q, send_sem, recv_sem):
-        return pltpu.make_async_remote_copy(
-            src_ref=part.at[d, :, lanes(q)],
-            dst_ref=near_in.at[which, d],
-            send_sem=send_sem.at[d],
-            recv_sem=recv_sem.at[d],
-            device_id=(s, near),
-            device_id_type=MESH,
-        )
-
-    def for_near(d):
-        return part_copy(d, 0, near, n0_send, n0_recv)
-
-    def for_diag(d):
-        return part_copy(d, 1, diag, n1_send, n1_recv)
-
-    def pair_copy(d):
-        return pltpu.make_async_remote_copy(
-            src_ref=pair.at[d],
-            dst_ref=far_in.at[d],
-            send_sem=g_send.at[d],
-            recv_sem=g_recv.at[d],
-            device_id=(s, far),
-            device_id_type=MESH,
-        )
-
-    def back(d):
-        return pltpu.make_async_remote_copy(
-            src_ref=total.at[d],
-            dst_ref=out.at[d],
-            send_sem=r_send.at[d],
-            recv_sem=r_recv.at[d],
-            device_id=((s + steps - d) % steps, t),
-            device_id_type=MESH,
-        )
-
-    def own_side():
-        return pltpu.make_async_copy(side, side_out.at[0], own_sem.at[2])
+    def weight_copies():
+        pairs = ((gate_held, w_gate), (up_held, w_up), (down_held, w_down))
+        return [pltpu.make_async_copy(a, b, own_sem.at[i]) for i, (a, b) in enumerate(pairs)]
+
+    def info_copy(dz):
+        peer = ((z + dz) % line) * 2 + y
+        return remote(info, infos.at[z], info_send.at[dz], info_recv.at[z], peer, t)
+
+    def info_from(zb):
+        return remote(info, infos.at[zb], info_send.at[0], info_recv.at[zb], across, t)
+
+    def line_copy(a, zb, src, up):
+        to = s + 2 if up else s - 2
+        return remote(src, tok.at[a, zb], line_send.at[a, up, zb], line_recv.at[a, zb], to, t)
+
+    def end_copy(a, zb, col, up):
+        to = s + 2 if up else s - 2
+        j = 2 * zb + y
+        if col == 0:
+            dst, recv = held.at[a, j, :, lanes(t)], arr_recv.at[a, j]
+        else:
+            dst, recv = cross.at[a, zb], cross_recv.at[a, zb]
+        return remote(over.at[a, zb, col], dst, end_send.at[a, col, zb], recv, to, t)
+
+    def across_copy(a, zb):
+        j = 2 * zb + y
+        dst = held.at[a, j, :, lanes(t)]
+        return remote(cross.at[a, zb], dst, across_send.at[a, zb], arr_recv.at[a, j], across, t)
+
+    def across_far(a):
+        dst = held.at[a, s, :, lanes(far)]
+        return remote(cross_far.at[a], dst, afar_send.at[a], far_recv.at[a, s], across, t)
+
+    def arrival(a, j):
+        place = held.at[a, j, :, lanes(t)]
+        return remote(place, place, f_send.at[a, j], arr_recv.at[a, j], s, far)
+
+    def to_tp(a, j, q, target, send_sem, recv_sem):
+        place = held.at[a, j, :, lanes(q)]
+        return remote(place, place, send_sem.at[a, j], recv_sem.at[a, j], s, target)
+
+    def near_copy(a, j):
+        return to_tp(a, j, t, near, b_send, near_recv)
+
+    def far_copy(a, j):
+        return to_tp(a, j, t, far, f_send, far_recv)
+
+    def fwd_copy(a, j):
+        return to_tp(a, j, far, near, c_send, fwd_recv)
+
+    def part_copy(j, which, q, send_sem, recv_sem):
+        src, dst = part.at[j, :, lanes(q)], near_in.at[which, j]
+        return remote(src, dst, send_sem.at[j], recv_sem.at[j], s, near)
+
+    def for_near(j):
+        return part_copy(j, 0, near, n0_send, n0_recv)
+
+    def for_diag(j):
+        return part_copy(j, 1, diag, n1_send, n1_recv)
+
+    def pair_copy(j):
+        return remote(pair.at[j], far_in.at[j], g_send.at[j], g_recv.at[j], s, far)
+
+    def back(j):
+        return remote(total.at[j], ret.at[s], r_send.at[j], r_recv.at[s], j, t)
+
+    def back_from(e):
+        return remote(total.at[e], ret.at[e], r_send.at[e], r_recv.at[e], e, t)
 
     def side_copy(d):
-        return pltpu.make_async_remote_copy(
-            src_ref=side,
-            dst_ref=side_out.at[d],
-            send_sem=s_send.at[d],
-            recv_sem=s_recv.at[d],
-            device_id=((s + d) % steps, t),
-            device_id_type=MESH,
-        )
-
-    def share(d):
-        for c in both:
-            to_sp(c, d).wait_recv()
-            far_copy(c, d).start()
-            near_copy(c, d).start()
-
-    def forward(d):
-        for c in both:
-            far_copy(c, d).wait_recv()
-            fwd_copy(c, d).start()
-
-    def arrived(d):
-        for c in both:
-            near_copy(c, d).wait_recv()
-            fwd_copy(c, d).wait_recv()
-
-    def experts(d):
-        gate_pre = jnp.dot(rows[d], w_gate[...], preferred_element_type=jnp.float32)
-        up_pre = jnp.dot(rows[d], w_up[...], preferred_element_type=jnp.float32)
-        act_grad = contract_cols(cots[d], w_down[...])
+        to = (s + d) % steps
+        return remote(side, side_out.at[d], s_send.at[d], s_recv.at[d], to, t)
+
+    def table(zb):
+        first, second = infos[zb, pl.ds(0, 1), :], infos[zb, pl.ds(1, 1), :]
+        ids = lax.broadcasted_iota(jnp.int32, (steps, tok_rows), 0).astype(jnp.float32)
+        chosen = (first == ids) | (second == ids)
+        ones = jnp.where(chosen, 1.0, 0.0).astype(kind)
+        rank = jnp.dot(ones, before[...], preferred_element_type=jnp.float32)
+        ranks[zb] = jnp.where(chosen, rank, -1.0)
+        weights[zb] = jnp.where(
+            first == ids, infos[zb, pl.ds(2, 1), :], infos[zb, pl.ds(3, 1), :]
+        )
+
+    def pick(zb, e):
+        slots = lax.broadcasted_iota(jnp.int32, (count, tok_rows), 0).astype(jnp.float32)
+        return slots == ranks[zb, pl.ds(e, 1), :]
+
+    def selected(a, zb, e, value):
+        mask = pick(zb, e)
+        hot = jnp.where(mask, 1.0, 0.0).astype(kind)
+        out = jnp.dot(hot, value, preferred_element_type=jnp.float32)
+        if a == 0:
+            scale = jnp.where(mask, weights[zb, pl.ds(e, 1), :], 0.0)
+            out = out * jnp.sum(scale, axis=1, keepdims=True)
+        return out.astype(kind)
+
+    def to_end(a, zb, value, up):
+        end = z + 1 if up else z - 1
+        for col in both:
+            e = 2 * end + (y if col == 0 else 1 - y)
+            over[a, zb, col] = selected(a, zb, e, value)
+            end_copy(a, zb, col, up).start()
+
+    def valid(m, up):
+        return (z >= m) if up else (z + m < line)
+
+    def block_at(m, up):
+        return z - m if up else z + m
+
+    def next_is_end(up):
+        return (z + 1 == line - 1) if up else (z == 1)
+
+    def next_is_inner(up):
+        return (z + 1 < line - 1) if up else (z >= 2)
+
+    def at_end(up):
+        return (z == line - 1) if up else (z == 0)
+
+    def share(a, j):
+        far_copy(a, j).start()
+        near_copy(a, j).start()
+
+    def read_info(m, up):
+        zb = block_at(m, up)
+
+        @pl.when(valid(m, up))
+        def _():
+            info_from(zb).wait_recv()
+
+        @pl.when(valid(m, up) & jnp.logical_not(at_end(up)))
+        def _():
+            table(zb)
+
+    def handle(a, m, up):
+        zb = block_at(m, up)
+        j = 2 * zb + y
+
+        @pl.when(valid(m, up) & at_end(up))
+        def _():
+            arrival(a, j).wait_recv()
+            end_copy(a, zb, 1, up).wait_recv()
+            across_copy(a, zb).start()
+            share(a, j)
+
+        @pl.when(valid(m, up) & jnp.logical_not(at_end(up)))
+        def _():
+            line_copy(a, zb, tok.at[a, zb], up).wait_recv()
+
+            @pl.when(next_is_end(up))
+            def _():
+                to_end(a, zb, tok[a, zb], up)
+
+            @pl.when(next_is_inner(up))
+            def _():
+                line_copy(a, zb, tok.at[a, zb], up).start()
+
+            cross[a, zb] = selected(a, zb, across, tok[a, zb])
+            across_copy(a, zb).start()
+            held[a, j, :, lanes(t)] = selected(a, zb, s, tok[a, zb])
+            share(a, j)
+
+    def each_block(m, body):
+        for up in both:
+            ok = valid(m, up) if up else valid(m, up) & (m > 0)
+
+            @pl.when(ok)
+            def _():
+                body(block_at(m, up))
+
+    def each_chunk(m, body):
+        def one(q):
+            up, other = q // 2, q % 2
+            zb = z + m - 2 * m * up
+            ok = (zb >= 0) & (zb < line) & ((m > 0) | (up == 1))
+
+            @pl.when(ok)
+            def _():
+                body(2 * zb + y + other * (1 - 2 * y))
+
+        looped(0, 4, one)
+
+    def unless_own(j, body):
+        @pl.when(j != s)
+        def _():
+            body()
+
+    def experts(j):
+        def settle():
+            for a in both:
+                near_copy(a, j).wait_recv()
+                fwd_copy(a, j).wait_recv()
+
+        unless_own(j, settle)
+        gate_pre = jnp.dot(held[1, j], w_gate[...], preferred_element_type=jnp.float32)
+        up_pre = jnp.dot(held[1, j], w_up[...], preferred_element_type=jnp.float32)
+        act_grad = contract_cols(held[0, j], w_down[...])
         gate_clamped = jnp.minimum(gate_pre, CLAMP_LIMIT)
         up_clamped = jnp.clip(up_pre, -CLAMP_LIMIT, CLAMP_LIMIT)
         sigma = jax.nn.sigmoid(SLOPE_ALPHA * gate_clamped)
         gated = gate_clamped * sigma
-        act[d] = ((up_clamped + 1.0) * gated).astype(jnp.bfloat16)
+        act[j] = ((up_clamped + 1.0) * gated).astype(kind)
         inside = (up_pre > -CLAMP_LIMIT) & (up_pre < CLAMP_LIMIT)
-        up_g = jnp.where(inside, act_grad * gated, 0.0).astype(jnp.bfloat16)
+        up_g = jnp.where(inside, act_grad * gated, 0.0).astype(kind)
         slope = sigma + SLOPE_ALPHA * gate_clamped * sigma * (1.0 - sigma)
         gate_g = jnp.where(
             gate_pre < CLAMP_LIMIT, act_grad * (up_clamped + 1.0) * slope, 0.0
-        ).astype(jnp.bfloat16)
-        gate_pg[d] = gate_g
-        up_pg[d] = up_g
-        for q in range(part.shape[-1] // width):
+        ).astype(kind)
+        gate_pg[j] = gate_g
+        up_pg[j] = up_g
+        for q in range(model_width // width):
             mine = pl.ds(q * width, width)
             value = contract_cols(gate_g, w_gate[mine, :]) + contract_cols(up_g, w_up[mine, :])
-            part[d, :, mine] = value.astype(part.dtype)
-
-    def open_up(d):
-        for_diag(d).start()
-        for_near(d).start()
-
-    def add_pair(d):
-        for_diag(d).wait_recv()
-        mine = part[d, :, lanes(far)].astype(jnp.float32)
-        pair[d] = (mine + near_in[1, d].astype(jnp.float32)).astype(pair.dtype)
-        pair_copy(d).start()
-
-    def whole(d):
-        for_near(d).wait_recv()
-        pair_copy(d).wait_recv()
-        mine = part[d, :, lanes(t)].astype(jnp.float32)
-        summed = mine + near_in[0, d].astype(jnp.float32)
-        return (summed + far_in[d].astype(jnp.float32)).astype(out.dtype)
-
-    def flat(ref, cols):
-        return ref[:, :, cols].reshape(-1, cols.size)
-
-    every = pl.ds(0, hidden)
+            part[j, :, mine] = value.astype(kind)
+        for_diag(j).start()
+        for_near(j).start()
+
+    def add_pair(j):
+        for_diag(j).wait_recv()
+        mine = part[j, :, lanes(far)].astype(jnp.float32)
+        pair[j] = (mine + near_in[1, j].astype(jnp.float32)).astype(kind)
+        pair_copy(j).start()
+
+    def whole(j):
+        for_near(j).wait_recv()
+        pair_copy(j).wait_recv()
+        mine = part[j, :, lanes(t)].astype(jnp.float32)
+        summed = mine + near_in[0, j].astype(jnp.float32)
+        return (summed + far_in[j].astype(jnp.float32)).astype(kind)
+
+    def send_back(j):
+        @pl.when(j == s)
+        def _():
+            ret[s] = whole(j)
+
+        @pl.when(j != s)
+        def _():
+            total[j] = whole(j)
+            back(j).start()
+
+    def forward(j):
+        def run():
+            for a in both:
+                far_copy(a, j).wait_recv()
+                fwd_copy(a, j).start()
+
+        unless_own(j, run)
+
+    def flat(value):
+        return value.reshape(-1, value.shape[-1])
 
     def row_grads(k):
         cols = pl.ds(pl.multiple_of(k * 256, 256), 256)
-        left = flat(rows, cols)
-        gate_grad[cols, :] = contract_rows(left, flat(gate_pg, every)).astype(gate_grad.dtype)
-        up_grad[cols, :] = contract_rows(left, flat(up_pg, every)).astype(up_grad.dtype)
+        left = flat(held[1, :, :, cols])
+        gate_grad[cols, :] = contract_rows(left, flat(gate_pg[...])).astype(kind)
+        up_grad[cols, :] = contract_rows(left, flat(up_pg[...])).astype(kind)
 
     def act_grads(k):
         cols = pl.ds(pl.multiple_of(k * 512, 512), 512)
-        down_grad[:, cols] = contract_rows(flat(act, every), flat(cots, cols)).astype(
-            down_grad.dtype
-        )
-
+        down_grad[:, cols] = contract_rows(flat(act[...]), flat(held[0, :, :, cols])).astype(kind)
+
+    for copy in weight_copies():
+        copy.start()
     meet(steps, True, near, far)
 
-    def send(k):
-        for c in both:
-            to_sp(c, k).start()
-
-    looped(1, steps, send)
-    own_side().start()
-    for c in both:
-        own(c).start()
-    for c in both:
-        own(c).wait()
+    def start_own(a):
+        src = sources[a]
+        for up in both:
+
+            @pl.when(next_is_inner(up))
+            def _():
+                line_copy(a, z, src.at[:, lanes(t)], up).start()
+
+    def end_own(a):
+        for up in both:
+
+            @pl.when(next_is_end(up))
+            def _():
+                to_end(a, z, sources[a][:, lanes(t)], up)
+
+    start_own(0)
+    looped(1, line, lambda dz: info_copy(dz).start())
+    infos[z] = info[...]
+    row_ids = lax.broadcasted_iota(jnp.int32, (tok_rows, tok_rows), 0)
+    col_ids = lax.broadcasted_iota(jnp.int32, (tok_rows, tok_rows), 1)
+    before[...] = jnp.where(row_ids < col_ids, 1.0, 0.0).astype(kind)
+    table(z)
+    end_own(0)
+    gain = norm_gain[...]
+
+    def normalise(k):
+        here = pl.ds(pl.multiple_of(k * 32, 32), 32)
+        x = resid[here, :].astype(jnp.float32)
+        scale = lax.rsqrt(jnp.mean(x * x, axis=-1, keepdims=True) + 1e-06)
+        normed[here, :] = (x * scale * gain).astype(kind)
+
+    looped(0, tok_rows // 32, normalise)
+    start_own(1)
+    end_own(1)
+    for a in both:
+        cross[a, z] = selected(a, z, across, sources[a][:, lanes(t)])
+        across_copy(a, z).start()
+        cross_far[a] = selected(a, z, across, sources[a][:, lanes(far)])
+        across_far(a).start()
+
+    def own_chunk(q):
+        for a in both:
+            held[a, s, :, lanes(q)] = selected(a, z, s, sources[a][:, lanes(q)])
+
+    looped(0, model_width // width, own_chunk)
+    summed = conv_sum[...].astype(jnp.float32)
+    centre = summed - jnp.mean(summed, axis=-1, keepdims=True)
+    inv_std = lax.rsqrt(jnp.mean(centre * centre, axis=-1, keepdims=True) + 1e-05)
+    pre_act = centre * inv_std * conv_gain[...]
+    conv_out = (pre_act * jax.nn.sigmoid(pre_act)).astype(kind)
+    side[...] = conv_out
+    side_out[0] = conv_out
+
+    def own_picks(e):
+        picks[e] = jnp.where(pick(z, e), 1.0, 0.0).astype(kind)
+
+    looped(0, steps, own_picks)
+    for copy in weight_copies():
+        copy.wait()
 
     def step(k):
-        @pl.when(k < steps)
+        @pl.when(k < line)
         def _():
-            share(k)
-            side_copy(k).start()
-
-        @pl.when((k >= 2) & (k < steps + 1))
+            for up in both:
+                read_info(k, up)
+            for a in both:
+                for up in both:
+                    handle(a, k, up)
+
+        @pl.when(k == line - 1)
         def _():
-            forward(k - 1)
-
-        @pl.when(k >= 3)
+            looped(1, steps, lambda d: side_copy(d).start())
+
+        @pl.when(k == 1)
         def _():
-            arrived(k - 2)
+            j = 2 * z + 1 - y
+            for a in both:
+                arrival(a, j).wait_recv()
+                near_copy(a, j).start()
+
+        each_chunk(k - 1, forward)
+        each_chunk(k - 1, experts)
+
+        @pl.when(k < line)
+        def _():
+            def meet_column(zb):
+                j = 2 * zb + 1 - y
+                for a in both:
+                    arrival(a, j).wait_recv()
+                    share(a, j)
+
+            each_block(k, meet_column)
+
+        each_chunk(k - 1, add_pair)
 
         @pl.when(k >= 2)
         def _():
-            experts(k - 2)
-            open_up(k - 2)
-
-        @pl.when(k >= 3)
+            each_chunk(k - 2, send_back)
+
+    looped(1, line + 1, step)
+    half = model_width // 512
+    looped(0, half, row_grads)
+    each_chunk(line - 1, send_back)
+    looped(half, 2 * half, row_grads)
+    looped(0, half, act_grads)
+
+    def gather_back(d):
+        back_from((s + d) % steps).wait_recv()
+
+    looped(1, steps, gather_back)
+    part_grad[...] = contract_rows(flat(picks[...]), flat(ret[...])).astype(kind)
+
+    def finish(j):
+        for_near(j).wait_send()
+        for_diag(j).wait_send()
+        pair_copy(j).wait_send()
+
+        @pl.when(j != s)
         def _():
-            add_pair(k - 3)
-
-        @pl.when(k >= 5)
+            back(j).wait_send()
+            for a in both:
+                near_copy(a, j).wait_send()
+                fwd_copy(a, j).wait_send()
+
+        @pl.when(j // 2 != z)
         def _():
-            d = k - 4
-            total[d] = whole(d)
-            back(d).start()
-
-    looped(1, steps + 2, step)
-    last = steps - 1
-    half = rows.shape[-1] // 512
-    looped(0, half, row_grads)
-    add_pair(last)
-    total[last - 1] = whole(last - 1)
-    back(last - 1).start()
-    looped(half, 2 * half, row_grads)
-    total[last] = whole(last)
-    back(last).start()
-    out[0] = whole(0)
-    looped(0, half, act_grads)
-
-    def finish(d):
-        for_near(d).wait_send()
-        for_diag(d).wait_send()
-        pair_copy(d).wait_send()
-
-    def finish_remote(d):
-        for c in both:
-            to_sp(c, d).wait_send()
-            near_copy(c, d).wait_send()
-            far_copy(c, d).wait_send()
-            fwd_copy(c, d).wait_send()
-        back(d).wait()
+            for a in both:
+                far_copy(a, j).wait_send()
+
+    looped(0, steps, finish)
+
+    def finish_side(d):
         side_copy(d).wait()
 
-    own_side().wait()
-    looped(0, steps, finish)
-    looped(1, steps, finish_remote)
-
-
-def routed_experts(
-    send_rows, send_cots, own_rows, own_cots, w_gate, w_up, w_down, side, collective_id
-):
-    steps, count, width = send_rows.shape
-    model_width, hidden = w_gate.shape
-    kind = send_rows.dtype
+    looped(1, steps, finish_side)
+    looped(1, line, lambda dz: info_copy(dz).wait_send())
+
+    def finish_line(m):
+        for up in both:
+            zb = block_at(m, up)
+
+            @pl.when(valid(m, up) & next_is_inner(up))
+            def _():
+                for a in both:
+                    line_copy(a, zb, tok.at[a, zb], up).wait_send()
+
+            @pl.when(valid(m, up) & next_is_end(up))
+            def _():
+                for a in both:
+                    for col in both:
+                        end_copy(a, zb, col, up).wait_send()
+
+    looped(0, line, finish_line)
+
+    def finish_across(zb):
+        for a in both:
+            across_copy(a, zb).wait_send()
+
+    looped(0, line, finish_across)
+    for a in both:
+        across_far(a).wait_send()
+
+
+def relay_experts(operands, collective_id):
+    info, resid, w_gate, conv_sum = operands[0], operands[2], operands[4], operands[7]
+    steps, tp_count = lax.axis_size("sp"), lax.axis_size("tp")
+    line = steps // 2
+    tok_rows, model_width = resid.shape
+    count = 3 * tok_rows // steps
+    width = model_width // tp_count
+    hidden = w_gate.shape[1]
+    kind = resid.dtype
     block = (steps, count, width)
     outs = [
         jax.ShapeDtypeStruct((model_width, hidden), kind),
         jax.ShapeDtypeStruct((model_width, hidden), kind),
         jax.ShapeDtypeStruct((hidden, model_width), kind),
-        jax.ShapeDtypeStruct(block, kind),
-        jax.ShapeDtypeStruct((steps,) + side.shape, side.dtype),
+        jax.ShapeDtypeStruct((tok_rows, width), kind),
+        jax.ShapeDtypeStruct((steps,) + conv_sum.shape, kind),
     ]
-    pairs = pltpu.SemaphoreType.DMA((2, steps))
-    ones = pltpu.SemaphoreType.DMA((steps,))
+    held = pl.BlockSpec(memory_space=pltpu.VMEM)
+    outside = pl.BlockSpec(memory_space=pl.ANY)
+
+    def sems(*shape):
+        return pltpu.SemaphoreType.DMA(shape)
+
     return pl.pallas_call(
-        functools.partial(routed_kernel, steps),
+        functools.partial(relay_kernel, steps),
         out_shape=tuple(outs),
-        in_specs=[pl.BlockSpec(memory_space=pltpu.VMEM)] * 8,
-        out_specs=tuple(pl.BlockSpec(memory_space=pltpu.VMEM) for _ in outs),
-        scratch_shapes=[pltpu.VMEM((steps, count, model_width), kind)] * 2
+        in_specs=[held] * 4 + [outside] * 3 + [held] * 2,
+        out_specs=tuple(held for _ in outs),
+        scratch_shapes=[
+            pltpu.VMEM((model_width, hidden), kind),
+            pltpu.VMEM((model_width, hidden), kind),
+            pltpu.VMEM((hidden, model_width), kind),
+            pltpu.VMEM((tok_rows, model_width), kind),
+            pltpu.VMEM((line,) + info.shape, jnp.float32),
+            pltpu.VMEM((line, steps, tok_rows), jnp.float32),
+            pltpu.VMEM((line, steps, tok_rows), jnp.float32),
+            pltpu.VMEM((tok_rows, tok_rows), kind),
+            pltpu.VMEM((steps, count, tok_rows), kind),
+            pltpu.VMEM((2, line, tok_rows, width), kind),
+            pltpu.VMEM((2, line, 2, count, width), kind),
+            pltpu.VMEM((2, line, count, width), kind),
+            pltpu.VMEM((2, count, width), kind),
+            pltpu.VMEM((2, steps, count, model_width), kind),
+        ]
         + [pltpu.VMEM((steps, count, hidden), kind)] * 3
         + [pltpu.VMEM((steps, count, model_width), kind), pltpu.VMEM((2,) + block, kind)]
-        + [pltpu.VMEM(block, kind)] * 3
-        + [pltpu.SemaphoreType.DMA((3,))]
-        + [pairs] * 8
-        + [ones] * 10,
+        + [pltpu.VMEM(block, kind)] * 4
+        + [pltpu.VMEM(conv_sum.shape, kind)]
+        + [sems(3), sems(line), sems(line), sems(2, 2, line), sems(2, line), sems(2, 2, line)]
+        + [sems(2, line), sems(2, line), sems(2), sems(2, steps)]
+        + [sems(2, steps)] * 6
+        + [sems(steps)] * 10,
         compiler_params=pltpu.CompilerParams(
-            collective_id=collective_id, has_side_effects=True, vmem_limit_bytes=36 << 20
+            collective_id=collective_id, has_side_effects=True, vmem_limit_bytes=42 << 20
         ),
-    )(send_rows, send_cots, own_rows, own_cots, w_gate, w_up, w_down, side)
+    )(*operands)
 
 
 def settle_kernel(
-    steps, part_grad, grad_out, resid, inv_rms, norm_gain, proj_weight,
+    steps, part_grad, grad_out, resid, norm_gain, proj_weight,
     conv_sum, conv_gain, conv_taps, conv_value, conv_gate,
     feature_cols, value_grad, gate_input_grad,
     full, grads, extended, far_send, far_recv, near_send, near_recv, fwd_send, fwd_recv,
@@ -740,7 +984,7 @@
         here = rows_of(j)
         feature_grad = full[here, :].astype(jnp.float32) * gain
         x = resid[here, :].astype(jnp.float32)
-        scale = inv_rms[here, :]
+        scale = lax.rsqrt(jnp.mean(x * x, axis=-1, keepdims=True) + 1e-06)
         cubed = scale * scale * scale
         mean = jnp.mean(x * feature_grad, axis=-1, keepdims=True)
         value = grad_out[here, :].astype(jnp.float32) + scale * feature_grad - x * cubed * mean
@@ -845,8 +1089,8 @@
 
 
 def settle_tokens(operands, collective_id):
-    part_grad, resid, conv_sum = operands[0], operands[2], operands[6]
-    overlap = operands[8].shape[0] - 1
+    part_grad, resid, conv_sum = operands[0], operands[2], operands[5]
+    overlap = operands[7].shape[0] - 1
     steps, tp_count = lax.axis_size("sp"), lax.axis_size("tp")
     tok_rows, model_width = resid.shape
     channels = conv_sum.shape[1]
@@ -879,11 +1123,9 @@
     )(*operands)
 
 
-def last_kernel(feature_cols, all_out, gate_in, up_in, down_in, proj, gate_out, up_out, down_out, sem):
-    moves = [
-        pltpu.make_async_copy(a, b, sem.at[i])
-        for i, (a, b) in enumerate(((gate_in, gate_out), (up_in, up_out), (down_in, down_out)))
-    ]
+def last_kernel(count, feature_cols, all_out, *refs):
+    ins, proj, outs, sem = refs[:count], refs[count], refs[count + 1 : -1], refs[-1]
+    moves = [pltpu.make_async_copy(a, b, sem.at[i]) for i, (a, b) in enumerate(zip(ins, outs))]
     for move in moves:
         move.start()
     proj[...] = contract_rows(feature_cols[...], all_out[...])
@@ -898,11 +1140,11 @@
     outs = [jax.ShapeDtypeStruct(shape, jnp.float32)]
     outs += [jax.ShapeDtypeStruct(g.shape, g.dtype) for g in grads]
     return pl.pallas_call(
-        last_kernel,
+        functools.partial(last_kernel, len(grads)),
         out_shape=tuple(outs),
-        in_specs=held * 5,
-        out_specs=tuple(held + outside * 3),
-        scratch_shapes=[pltpu.SemaphoreType.DMA((3,))],
+        in_specs=held * (2 + len(grads)),
+        out_specs=tuple(held + outside * len(grads)),
+        scratch_shapes=[pltpu.SemaphoreType.DMA((len(grads),))],
         compiler_params=pltpu.CompilerParams(vmem_limit_bytes=16 << 20),
     )(feature_cols, all_out, *grads)
 
@@ -928,6 +1170,42 @@
     tp_count = lax.axis_size("tp")
     capacity = 3 * tok_rows // sp_count
     col_count = model_width // tp_count
+    channels = conv_sum.shape[1]
+    aligned = capacity % 16 == 0 and model_width % (128 * sp_count) == 0 and channels == GROUP
+    if aligned and sp_count % 4 == 0:
+        side_rows = (routes.T.astype(jnp.float32), route_weights.T)
+        info = jnp.pad(jnp.concatenate(side_rows, axis=0), ((0, 4), (0, 0)))
+        operands = (
+            info,
+            grad_out,
+            resid,
+            norm_gain[None],
+            gate_weight[0],
+            up_weight[0],
+            down_weight[0],
+            conv_sum,
+            conv_gain[None],
+        )
+        gate_grad, up_grad, down_grad, part_grad, all_out = relay_experts(operands, 4)
+        operands = (
+            part_grad,
+            grad_out,
+            resid,
+            norm_gain[None],
+            proj_weight,
+            conv_sum,
+            conv_gain[None],
+            conv_taps,
+            conv_value,
+            conv_gate,
+        )
+        feature_cols, value_grad, gate_input_grad = settle_tokens(operands, 5)
+        proj_grad, *ends = last_stage(
+            feature_cols.reshape(sp_count * tok_rows, model_width // sp_count),
+            all_out.reshape(sp_count * tok_rows, channels),
+            (gate_grad, up_grad, down_grad, value_grad, gate_input_grad),
+        )
+        return tuple(g[None] for g in ends[:3]) + (proj_grad,) + tuple(ends[3:])
     resid_f = resid.astype(jnp.float32)
     inv_rms = lax.rsqrt(jnp.mean(resid_f * resid_f, axis=-1, keepdims=True) + 1e-06)
     normed = (resid_f * inv_rms * norm_gain).astype(jnp.bfloat16)
@@ -956,7 +1234,6 @@
     own_rows = jnp.dot(own_pick, normed, preferred_element_type=jnp.float32).astype(jnp.bfloat16)
     own_cots = jnp.dot(own_pick, grad_out, preferred_element_type=jnp.float32)
     own_cots = (own_cots * slot_weight[:capacity]).astype(jnp.bfloat16)
-    channels = conv_sum.shape[1]
     summed = conv_sum.astype(jnp.float32).reshape(tok_rows, channels // GROUP, GROUP)
     centre = summed - jnp.mean(summed, axis=-1, keepdims=True)
     inv_std = lax.rsqrt(jnp.mean(centre * centre, axis=-1, keepdims=True) + 1e-05)
@@ -965,64 +1242,26 @@
     pre_act = chan_normed * conv_gain
     sigma_conv = jax.nn.sigmoid(pre_act)
     conv_out = (pre_act * sigma_conv).astype(jnp.bfloat16)
-    aligned = capacity % 16 == 0 and model_width % (128 * sp_count) == 0 and channels == GROUP
-    if aligned:
-        gate_grad, up_grad, down_grad, returned, all_out = routed_experts(
+    routed_rows, routed_cots = spread(
+        (
             send_rows.reshape(sp_count, capacity, col_count),
             send_cots.reshape(sp_count, capacity, col_count),
-            own_rows,
-            own_cots,
-            gate_weight[0],
-            up_weight[0],
-            down_weight[0],
-            conv_out,
-            4,
-        )
-        returned = returned.reshape(sp_count * capacity, col_count)
-    else:
-        routed_rows, routed_cots = spread(
-            (
-                send_rows.reshape(sp_count, capacity, col_count),
-                send_cots.reshape(sp_count, capacity, col_count),
-            ),
-            (own_rows, own_cots),
-            None,
-            True,
-            False,
-            0,
-        )
-        routed_rows = routed_rows.reshape(sp_count * capacity, model_width)
-        routed_cots = routed_cots.reshape(sp_count * capacity, model_width)
-        gate_grad, up_grad, down_grad, partial_value = expert_backward(
-            routed_rows, routed_cots, gate_weight[0], up_weight[0], down_weight[0]
-        )
-        returned = combine(
-            partial_value.reshape(sp_count, capacity, model_width).astype(jnp.bfloat16), 1
-        ).reshape(sp_count * capacity, col_count)
+        ),
+        (own_rows, own_cots),
+        None,
+        True,
+        False,
+        0,
+    )
+    routed_rows = routed_rows.reshape(sp_count * capacity, model_width)
+    routed_cots = routed_cots.reshape(sp_count * capacity, model_width)
+    gate_grad, up_grad, down_grad, partial_value = expert_backward(
+        routed_rows, routed_cots, gate_weight[0], up_weight[0], down_weight[0]
+    )
+    returned = combine(
+        partial_value.reshape(sp_count, capacity, model_width).astype(jnp.bfloat16), 1
+    ).reshape(sp_count * capacity, col_count)
     normed_part_grad = contract_rows(pick, returned).astype(jnp.bfloat16)
-    if aligned:
-        operands = (
-            normed_part_grad,
-            grad_out,
-            resid,
-            inv_rms,
-            norm_gain[None],
-            proj_weight,
-            conv_sum,
-            conv_gain[None],
-            conv_taps,
-            conv_value,
-            conv_gate,
-        )
-        feature_cols, value_grad, gate_input_grad = settle_tokens(operands, 5)
-        feat_rows = model_width // sp_count
-        proj_grad, gate_grad, up_grad, down_grad = last_stage(
-            feature_cols.reshape(sp_count * tok_rows, feat_rows),
-            all_out.reshape(sp_count * tok_rows, channels),
-            (gate_grad, up_grad, down_grad),
-        )
-        weight_grads = (gate_grad[None], up_grad[None], down_grad[None])
-        return weight_grads + (proj_grad, value_grad, gate_input_grad)
     chunks = 4
     normed_grad, all_out = spread(
         (normed_part_grad.reshape(chunks, tok_rows // chunks, col_count),),

time: 131 us -> 120 us (0.916)
  Pallas kernels: 118 us -> 108 us
  other arithmetic: 6.81 us -> 1.37 us
  local copies, waits for them, and re-layouts: 3.77 us -> 8.88 us
  matrix products: 1.98 us -> 0 us
    pallas_call x2, Pallas kernels: 94.5 us -> 82.4 us  [the longest x1 79.4 us: relay_experts(): pl.pallas_call(functools.partial(relay_kernel, steps), out_shape=tuple(ou...]
    unnamed x26 -> x24, local copies, waits for them, and re-layouts: 3.48 us -> 8.88 us
    reduce_sum x5 -> x0, other arithmetic: 4.5 us -> none  [the longest x1 1.6 us: local(): jnp.mean(resid_f * resid_f, axis=-1, keepdims=True) + 1e-06]
    pallas_call x1, Pallas kernels: 23 us -> 25.8 us  [settle_tokens(): pl.pallas_call(functools.partial(settle_kernel, steps), out_shape=tuple(o...]
    dot_general x6 -> x0, matrix products: 1.98 us -> none  [the longest x1 0.42 us: contract_rows(): lax.dot_general(left_side, right_side, (((0,), (0,)), ((), ())), preferre...]
where the time goes in v3:
time: 120 us; the launch traced here: 119 us
  Pallas kernels  108 us (90%)
  local copies, waits for them, and re-layouts  8.88 us (7%)
  other arithmetic  1.37 us (1%)
    pallas_call x1, Pallas kernels, relay_experts(): pl.pallas_call(functools.partial(relay_kernel, steps), out_shape=tuple(ou...  79.4 us
    pallas_call x1, Pallas kernels, settle_tokens(): pl.pallas_call(functools.partial(settle_kernel, steps), out_shape=tuple(o...  25.8 us
    unnamed x24, local copies, waits for them, and re-layouts  8.88 us
    pallas_call x1, Pallas kernels, last_stage(): pl.pallas_call(functools.partial(last_kernel, len(grads)), out_shape=tupl...  3.06 us

profile of v3, /device:TPU:0, one launch (start us, length us, event | category | flops | bytes accessed | tf_op | source)
XLA Modules:
  0.0 119.2 jit_solution(5256037198768618191)
XLA Ops:
  0.6 0.7 convert_bitcast_fusion
  1.3 0.7 select_maximum_fusion.info
  2.0 0.0 copy-start
  2.0 1.2 %copy-done = bf16[256,2048]{1,0:T(8,128)(2,1)S(1)} copy-done((bf16[256,2048]{1,0:T(8,128)(2,1)S(1)}, bf16[256,2048]{1,0:T(8,128)(2,1)}, u32[]{:S(2)}) %copy-start) | copy-done | bytes 1048600
  3.2 0.0 copy-start.1
  3.2 1.2 %copy-done.1 = bf16[256,2048]{1,0:T(8,128)(2,1)S(1)} copy-done((bf16[256,2048]{1,0:T(8,128)(2,1)S(1)}, bf16[256,2048]{1,0:T(8,128)(2,1)}, u32[]{:S(2)}) %copy-start.1) | copy-done | bytes 1048600
  4.5 0.0 copy-start.2
  4.5 1.4 %copy-done.2 = bf16[1,2048,384]{2,1,0:T(8,128)(2,1)S(1)} copy-done((bf16[1,2048,384]{2,1,0:T(8,128)(2,1)S(1)}, bf16[1,2048,384]{2,1,0:T(8,128)(2,1)}, u32[]{:S(2)}) %copy-start.2) | copy-done | bytes 1572888
  5.9 0.0 copy-start.3
  5.9 1.4 %copy-done.3 = bf16[1,2048,384]{2,1,0:T(8,128)(2,1)S(1)} copy-done((bf16[1,2048,384]{2,1,0:T(8,128)(2,1)S(1)}, bf16[1,2048,384]{2,1,0:T(8,128)(2,1)}, u32[]{:S(2)}) %copy-start.3) | copy-done | bytes 1572888
  7.3 0.0 copy-start.4
  7.3 1.4 %copy-done.4 = bf16[1,384,2048]{2,1,0:T(8,128)(2,1)S(1)} copy-done((bf16[1,384,2048]{2,1,0:T(8,128)(2,1)S(1)}, bf16[1,384,2048]{2,1,0:T(8,128)(2,1)}, u32[]{:S(2)}) %copy-start.4) | copy-done | bytes 1572888
  8.7 0.0 copy-start.6
  8.7 0.8 copy-done.6
  9.5 0.0 copy-start.9
  9.5 0.7 copy-done.9
  10.2 0.7 copy-done.11
  10.9 79.4 %shard_map.181 = (bf16[2048,384]{1,0:T(8,128)(2,1)S(1)}, bf16[2048,384]{1,0:T(8,128)(2,1)S(1)}, bf16[384,2048]{1,0:T(8,128)(2,1)S(1)}, bf16[256,512]{1,0:T(8,128)(2,1)S(1)}, bf16[8,256,128]{2,1,0:T(8,128)(2,1)S(1)}) custom-call(f32[8,256]{1,0:T(8,128)S(1)} %select_maximum_fusion.info, bf16[256,2048]{1,0:T(8,128)(2,1)S(1)} %copy-done, ...), custom_call_target="tpu_custom_call" | custom-call | tf_op jit(solution)/shard_map/pallas_call | solution.py:860
  90.3 0.0 copy-done.5
  90.3 0.0 copy-done.7
  90.3 0.0 copy-done.8
  90.3 0.0 copy-done.10
  90.3 25.8 %shard_map.182 = (bf16[8,4,64,256]{3,2,1,0:T(8,128)(2,1)S(1)}, bf16[256,128]{1,0:T(8,128)(2,1)S(1)}, bf16[256,128]{1,0:T(8,128)(2,1)S(1)}) custom-call(bf16[256,512]{1,0:T(8,128)(2,1)S(1)} %get-tuple-element.20.part_grad, bf16[256,2048]{1,0:T(8,128)(2,1)S(1)} %copy-done, bf16[256,2048]{1,0:T(8,128)(2,1)S(1)} %copy-done.1, f32[1,2048]{1,0:T(1,128)S(1)} %bitcast.19, ...), custom_call_target="tpu_custom_call" | custom-call | tf_op jit(solution)/shard_map/pallas_call | solution.py:1106
  116.1 3.1 %shard_map.183 = (f32[256,128]{1,0:T(8,128)}, bf16[2048,384]{1,0:T(8,128)(2,1)}, bf16[2048,384]{1,0:T(8,128)(2,1)}, bf16[384,2048]{1,0:T(8,128)(2,1)}, bf16[256,...) custom-call(bf16[2048,256]{1,0:T(8,128)(2,1)S(1)} %bitcast.16, bf16[2048,128]{1,0:T(8,128)(2,1)S(1)} %bitcast.17, ...), custom_call_target="tpu_custom_call" | custom-call | tf_op jit(solution)/shard_map/pallas_call | solution.py:1142
  (5 shorter events, 0.0 us)
Async XLA Ops:
  2.0 1.2 %copy-start = (bf16[256,2048]{1,0:T(8,128)(2,1)S(1)}, bf16[256,2048]{1,0:T(8,128)(2,1)}, u32[]{:S(2)}) copy-start(bf16[256,2048]{1,0:T(8,128)(2,1)} %grad_out.3) | copy-start | bytes 3145732
  3.2 1.2 %copy-start.1 = (bf16[256,2048]{1,0:T(8,128)(2,1)S(1)}, bf16[256,2048]{1,0:T(8,128)(2,1)}, u32[]{:S(2)}) copy-start(bf16[256,2048]{1,0:T(8,128)(2,1)} %resid.3) | copy-start | bytes 3145732
  4.5 1.4 %copy-start.2 = (bf16[1,2048,384]{2,1,0:T(8,128)(2,1)S(1)}, bf16[1,2048,384]{2,1,0:T(8,128)(2,1)}, u32[]{:S(2)}) copy-start(bf16[1,2048,384]{2,1,0:T(8,128)(2,1)} %param.19) | copy-start | bytes 4718596
  5.9 1.4 %copy-start.3 = (bf16[1,2048,384]{2,1,0:T(8,128)(2,1)S(1)}, bf16[1,2048,384]{2,1,0:T(8,128)(2,1)}, u32[]{:S(2)}) copy-start(bf16[1,2048,384]{2,1,0:T(8,128)(2,1)} %param.20) | copy-start | bytes 4718596
  7.3 1.4 %copy-start.4 = (bf16[1,384,2048]{2,1,0:T(8,128)(2,1)S(1)}, bf16[1,384,2048]{2,1,0:T(8,128)(2,1)}, u32[]{:S(2)}) copy-start(bf16[1,384,2048]{2,1,0:T(8,128)(2,1)} %param.21) | copy-start | bytes 4718596
  8.7 0.8 copy-start.6
  9.5 0.7 copy-start.9
  10.2 0.7 copy-start.11
  10.9 79.4 %copy-start.5 = (bf16[2048,128]{1,0:T(8,128)(2,1)S(1)}, bf16[2048,128]{1,0:T(8,128)(2,1)}, u32[]{:S(2)}) copy-start(bf16[2048,128]{1,0:T(8,128)(2,1)} %proj_weight.1) | copy-start | bytes 1572868
  10.9 79.4 %copy-start.7 = (bf16[256,128]{1,0:T(8,128)(2,1)S(1)}, bf16[256,128]{1,0:T(8,128)(2,1)}, u32[]{:S(2)}) copy-start(bf16[256,128]{1,0:T(8,128)(2,1)} %conv_value.1) | copy-start | bytes 196612
  10.9 79.4 %copy-start.8 = (bf16[256,128]{1,0:T(8,128)(2,1)S(1)}, bf16[256,128]{1,0:T(8,128)(2,1)}, u32[]{:S(2)}) copy-start(bf16[256,128]{1,0:T(8,128)(2,1)} %conv_gate.1) | copy-start | bytes 196612
  10.9 79.4 %copy-start.10 = (f32[31,128]{1,0:T(8,128)S(1)}, f32[31,128]{1,0:T(8,128)}, u32[]{:S(2)}) copy-start(f32[31,128]{1,0:T(8,128)} %conv_taps.1) | copy-start | bytes 47620

commit v4 on v3

--- a/solution.py
+++ b/solution.py
@@ -370,10 +370,35 @@
     return (gate_grad, up_grad, down_grad, partial_value)
 
 
+def line_schedule(line):
+    codes = []
+    for z in range(line):
+        slots = [[(z, 0), 0, 0, 0], [(z, 1), 1, 1, 0]]
+        groups = [[b for b in (z - k, z + k) if 0 <= b < line] for k in range(1, line)]
+        groups = [g for g in groups if g]
+        for k, group in enumerate(groups, 1):
+            following = k + 1 if k < len(groups) else 0
+            added = [[(b, 0), 0, 0, 0] for b in group] + [[(b, 1), 0, 0, 0] for b in group]
+            many = len(group)
+            added[0][3] = group[0] + 1
+            if many > 1:
+                added[many][3] = group[1] + 1
+            added[1][1] = following
+            added[many][2] = following
+            slots += added
+        row = []
+        for (zb, col), first, second, meeting in slots:
+            row.append((((meeting * 16 + second) * 16 + first) * 2 + col) * 16 + zb)
+        codes.append(row)
+    return codes
+
+
 def relay_kernel(
-    steps, info, grad_out, resid, norm_gain, gate_held, up_held, down_held, conv_sum, conv_gain,
+    steps, routes_in, weights_in, grad_in, resid_in, gain_in, gate_in, up_in, down_in, sum_in,
+    conv_gain_in,
     gate_grad, up_grad, down_grad, part_grad, side_out,
-    w_gate, w_up, w_down, normed, infos, ranks, weights, before, picks,
+    routes, route_weights, grad_out, resid, norm_gain, w_gate, w_up, w_down, conv_sum, conv_gain,
+    normed, info, infos, ranks, weights, before, picks,
     tok, over, cross, cross_far, held, act, gate_pg, up_pg, part,
     near_in, pair, far_in, total, ret, side,
     own_sem, info_send, info_recv, line_send, line_recv, end_send, cross_recv,
@@ -406,9 +431,23 @@
             device_id_type=MESH,
         )
 
-    def weight_copies():
-        pairs = ((gate_held, w_gate), (up_held, w_up), (down_held, w_down))
-        return [pltpu.make_async_copy(a, b, own_sem.at[i]) for i, (a, b) in enumerate(pairs)]
+    moves = [
+        pltpu.make_async_copy(a, b, own_sem.at[i])
+        for i, (a, b) in enumerate(
+            (
+                (grad_in, grad_out),
+                (routes_in, routes),
+                (weights_in, route_weights),
+                (resid_in, resid),
+                (gain_in, norm_gain),
+                (sum_in, conv_sum),
+                (conv_gain_in, conv_gain),
+                (gate_in, w_gate),
+                (up_in, w_up),
+                (down_in, w_down),
+            )
+        )
+    ]
 
     def info_copy(dz):
         peer = ((z + dz) % line) * 2 + y
@@ -567,26 +606,6 @@
             across_copy(a, zb).start()
             held[a, j, :, lanes(t)] = selected(a, zb, s, tok[a, zb])
             share(a, j)
-
-    def each_block(m, body):
-        for up in both:
-            ok = valid(m, up) if up else valid(m, up) & (m > 0)
-
-            @pl.when(ok)
-            def _():
-                body(block_at(m, up))
-
-    def each_chunk(m, body):
-        def one(q):
-            up, other = q // 2, q % 2
-            zb = z + m - 2 * m * up
-            ok = (zb >= 0) & (zb < line) & ((m > 0) | (up == 1))
-
-            @pl.when(ok)
-            def _():
-                body(2 * zb + y + other * (1 - 2 * y))
-
-        looped(0, 4, one)
 
     def unless_own(j, body):
         @pl.when(j != s)
@@ -667,9 +686,10 @@
         cols = pl.ds(pl.multiple_of(k * 512, 512), 512)
         down_grad[:, cols] = contract_rows(flat(act[...]), flat(held[0, :, :, cols])).astype(kind)
 
-    for copy in weight_copies():
-        copy.start()
+    for move in moves:
+        move.start()
     meet(steps, True, near, far)
+    moves[0].wait()
 
     def start_own(a):
         src = sources[a]
@@ -687,13 +707,19 @@
                 to_end(a, z, sources[a][:, lanes(t)], up)
 
     start_own(0)
+    moves[1].wait()
+    moves[2].wait()
+    info[pl.ds(0, 2), :] = routes[...].astype(jnp.float32)
+    info[pl.ds(2, 2), :] = route_weights[...]
+    infos[z] = info[...]
     looped(1, line, lambda dz: info_copy(dz).start())
-    infos[z] = info[...]
     row_ids = lax.broadcasted_iota(jnp.int32, (tok_rows, tok_rows), 0)
     col_ids = lax.broadcasted_iota(jnp.int32, (tok_rows, tok_rows), 1)
     before[...] = jnp.where(row_ids < col_ids, 1.0, 0.0).astype(kind)
     table(z)
     end_own(0)
+    for move in moves[3:5]:
+        move.wait()
     gain = norm_gain[...]
 
     def normalise(k):
@@ -716,6 +742,8 @@
             held[a, s, :, lanes(q)] = selected(a, z, s, sources[a][:, lanes(q)])
 
     looped(0, model_width // width, own_chunk)
+    for move in moves[5:7]:
+        move.wait()
     summed = conv_sum[...].astype(jnp.float32)
     centre = summed - jnp.mean(summed, axis=-1, keepdims=True)
     inv_std = lax.rsqrt(jnp.mean(centre * centre, axis=-1, keepdims=True) + 1e-05)
@@ -728,54 +756,89 @@
         picks[e] = jnp.where(pick(z, e), 1.0, 0.0).astype(kind)
 
     looped(0, steps, own_picks)
-    for copy in weight_copies():
-        copy.wait()
-
-    def step(k):
-        @pl.when(k < line)
+    for move in moves[7:]:
+        move.wait()
+
+    codes = line_schedule(line)
+    middle = steps // 2
+
+    def slot_code(n):
+        code = 0
+        for zz in range(line):
+            for nn in range(steps):
+                code = code + jnp.where((z == zz) & (n == nn), codes[zz][nn], 0)
+        return code
+
+    def chunk_at(n):
+        code = slot_code(n)
+        other = (code // 16) % 2
+        return 2 * (code % 16) + y + other * (1 - 2 * y)
+
+    def slot(n):
+        code = slot_code(n)
+        zb, other = code % 16, (code // 16) % 2
+        first, second = (code // 32) % 16, (code // 512) % 16
+        meeting = code // 8192
+        j = 2 * zb + y + other * (1 - 2 * y)
+
+        @pl.when(meeting > 0)
+        def _():
+            met = 2 * (meeting - 1) + 1 - y
+            for a in both:
+                arrival(a, met).wait_recv()
+                share(a, met)
+
+        @pl.when(first > 0)
         def _():
             for up in both:
-                read_info(k, up)
-            for a in both:
-                for up in both:
-                    handle(a, k, up)
-
-        @pl.when(k == line - 1)
-        def _():
-            looped(1, steps, lambda d: side_copy(d).start())
-
-        @pl.when(k == 1)
-        def _():
-            j = 2 * z + 1 - y
+                read_info(first, up)
+            for up in both:
+                handle(0, first, up)
+
+        @pl.when(second > 0)
+        def _():
+            for up in both:
+                handle(1, second, up)
+
+        @pl.when(n == 1)
+        def _():
             for a in both:
                 arrival(a, j).wait_recv()
                 near_copy(a, j).start()
 
-        each_chunk(k - 1, forward)
-        each_chunk(k - 1, experts)
-
-        @pl.when(k < line)
-        def _():
-            def meet_column(zb):
-                j = 2 * zb + 1 - y
-                for a in both:
-                    arrival(a, j).wait_recv()
-                    share(a, j)
-
-            each_block(k, meet_column)
-
-        each_chunk(k - 1, add_pair)
-
-        @pl.when(k >= 2)
-        def _():
-            each_chunk(k - 2, send_back)
-
-    looped(1, line + 1, step)
+        @pl.when(n == steps - 2)
+        def _():
+            looped(1, steps, lambda d: side_copy(d).start())
+
+        forward(j)
+        experts(j)
+
+        @pl.when(n == 0)
+        def _():
+            add_pair(j)
+
+        @pl.when(n > middle)
+        def _():
+            add_pair(chunk_at(n - 1))
+
+    def pair_at(n):
+        add_pair(chunk_at(n))
+
+    def back_at(n):
+        send_back(chunk_at(n))
+
+    looped(0, steps, slot)
     half = model_width // 512
+    pair_at(steps - 1)
+    looped(1, middle, pair_at)
+    looped(middle, steps - 2, back_at)
     looped(0, half, row_grads)
-    each_chunk(line - 1, send_back)
+    back_at(steps - 2)
     looped(half, 2 * half, row_grads)
+    back_at(steps - 1)
     looped(0, half, act_grads)
+    looped(1, middle, back_at)
+    back_at(0)
 
     def gather_back(d):
         back_from((s + d) % steps).wait_recv()
@@ -835,7 +898,7 @@
 
 
 def relay_experts(operands, collective_id):
-    info, resid, w_gate, conv_sum = operands[0], operands[2], operands[4], operands[7]
+    routes, resid, w_gate, conv_sum = operands[0], operands[3], operands[5], operands[8]
     steps, tp_count = lax.axis_size("sp"), lax.axis_size("tp")
     line = steps // 2
     tok_rows, model_width = resid.shape
@@ -852,7 +915,7 @@
         jax.ShapeDtypeStruct((steps,) + conv_sum.shape, kind),
     ]
     held = pl.BlockSpec(memory_space=pltpu.VMEM)
-    outside = pl.BlockSpec(memory_space=pl.ANY)
+    outside = pl.BlockSpec(memory_space=pltpu.HBM)
 
     def sems(*shape):
         return pltpu.SemaphoreType.DMA(shape)
@@ -860,14 +923,13 @@
     return pl.pallas_call(
         functools.partial(relay_kernel, steps),
         out_shape=tuple(outs),
-        in_specs=[held] * 4 + [outside] * 3 + [held] * 2,
+        in_specs=[outside] * len(operands),
         out_specs=tuple(held for _ in outs),
-        scratch_shapes=[
-            pltpu.VMEM((model_width, hidden), kind),
-            pltpu.VMEM((model_width, hidden), kind),
-            pltpu.VMEM((hidden, model_width), kind),
+        scratch_shapes=[pltpu.VMEM(x.shape, x.dtype) for x in operands]
+        + [
             pltpu.VMEM((tok_rows, model_width), kind),
-            pltpu.VMEM((line,) + info.shape, jnp.float32),
+            pltpu.VMEM((2 * routes.shape[0], tok_rows), jnp.float32),
+            pltpu.VMEM((line, 2 * routes.shape[0], tok_rows), jnp.float32),
             pltpu.VMEM((line, steps, tok_rows), jnp.float32),
             pltpu.VMEM((line, steps, tok_rows), jnp.float32),
             pltpu.VMEM((tok_rows, tok_rows), kind),
@@ -882,14 +944,14 @@
         + [pltpu.VMEM((steps, count, model_width), kind), pltpu.VMEM((2,) + block, kind)]
         + [pltpu.VMEM(block, kind)] * 4
         + [pltpu.VMEM(conv_sum.shape, kind)]
-        + [sems(3), sems(line), sems(line), sems(2, 2, line), sems(2, line), sems(2, 2, line)]
+        + [sems(len(operands)), sems(line), sems(line), sems(2, 2, line), sems(2, line), sems(2, 2, line)]
         + [sems(2, line), sems(2, line), sems(2), sems(2, steps)]
         + [sems(2, steps)] * 6
         + [sems(steps)] * 10,
         compiler_params=pltpu.CompilerParams(
             collective_id=collective_id, has_side_effects=True, vmem_limit_bytes=42 << 20
         ),
-    )(*operands)
+    )(*(pltpu.with_memory_space_constraint(x, pltpu.HBM) for x in operands))
 
 
 def settle_kernel(
@@ -1173,10 +1235,9 @@
     channels = conv_sum.shape[1]
     aligned = capacity % 16 == 0 and model_width % (128 * sp_count) == 0 and channels == GROUP
     if aligned and sp_count % 4 == 0:
-        side_rows = (routes.T.astype(jnp.float32), route_weights.T)
-        info = jnp.pad(jnp.concatenate(side_rows, axis=0), ((0, 4), (0, 0)))
         operands = (
-            info,
+            routes.T,
+            route_weights.T,
             grad_out,
             resid,
             norm_gain[None],

time: 120 us -> 107 us (0.89)
  local copies, waits for them, and re-layouts: 8.88 us -> 0.04 us
  Pallas kernels: 108 us -> 106 us
  other arithmetic: 1.37 us -> 0 us
    unnamed x24 -> x18, local copies, waits for them, and re-layouts: 8.88 us -> 0.04 us
    pallas_call x1, Pallas kernels: 79.4 us -> 77.6 us  [relay_experts(): pl.pallas_call(functools.partial(relay_kernel, steps), out_shape=tuple(ou...]
where the time goes in v4:
time: 107 us
  Pallas kernels  106 us (99%)
    pallas_call x1, Pallas kernels, relay_experts(): pl.pallas_call(functools.partial(relay_kernel, steps), out_shape=tuple(ou...  77.6 us
    pallas_call x1, Pallas kernels, settle_tokens(): pl.pallas_call(functools.partial(settle_kernel, steps), out_shape=tuple(o...  25.4 us
    pallas_call x1, Pallas kernels, last_stage(): pl.pallas_call(functools.partial(last_kernel, len(grads)), out_shape=tupl...  3.07 us

profile of v4, /device:TPU:0, one launch (start us, length us, event | category | flops | bytes accessed | tf_op | source)
XLA Modules:
  0.0 106.9 jit_solution(12393125569654599174)
XLA Ops:
  0.6 0.0 copy-start
  0.6 0.0 copy-start.1
  0.7 0.0 copy-start.2
  0.7 0.0 copy-start.3
  0.7 0.0 copy-start.4
  0.7 0.0 copy-start.5
  0.7 0.0 copy-start.6
  0.7 0.0 copy-start.7
  0.7 0.0 copy-start.8
  0.7 77.6 %shard_map.181 = (bf16[2048,384]{1,0:T(8,128)(2,1)S(1)}, bf16[2048,384]{1,0:T(8,128)(2,1)S(1)}, bf16[384,2048]{1,0:T(8,128)(2,1)S(1)}, bf16[256,512]{1,0:T(8,128)(2,1)S(1)}, bf16[8,256,128]{2,1,0:T(8,128)(2,1)S(1)}) custom-call(s32[2,256]{1,0:T(2,128)} %bitcast.21, f32[2,256]{1,0:T(2,128)} %bitcast.22, bf16[256,2048]{1,0:T(8,128)(2,1)} %grad_out.1, ...), custom_call_target="tpu_custom_call" | custom-call | tf_op jit(solution)/shard_map/pallas_call | solution.py:923
  78.3 0.0 copy-done
  78.3 0.0 copy-done.1
  78.4 0.0 copy-done.2
  78.4 0.0 copy-done.3
  78.4 0.0 copy-done.4
  78.4 0.0 copy-done.5
  78.4 0.0 copy-done.6
  78.4 0.0 copy-done.7
  78.4 0.0 copy-done.8
  78.4 25.4 %shard_map.182 = (bf16[8,4,64,256]{3,2,1,0:T(8,128)(2,1)S(1)}, bf16[256,128]{1,0:T(8,128)(2,1)S(1)}, bf16[256,128]{1,0:T(8,128)(2,1)S(1)}) custom-call(bf16[256,512]{1,0:T(8,128)(2,1)S(1)} %get-tuple-element.20.part_grad, bf16[256,2048]{1,0:T(8,128)(2,1)S(1)} %copy-done, bf16[256,2048]{1,0:T(8,128)(2,1)S(1)} %copy-done.1, f32[1,2048]{1,0:T(1,128)S(1)} %bitcast.15, ...), custom_call_target="tpu_custom_call" | custom-call | tf_op jit(solution)/shard_map/pallas_call | solution.py:1168
  103.8 3.1 %shard_map.183 = (f32[256,128]{1,0:T(8,128)}, bf16[2048,384]{1,0:T(8,128)(2,1)}, bf16[2048,384]{1,0:T(8,128)(2,1)}, bf16[384,2048]{1,0:T(8,128)(2,1)}, bf16[256,...) custom-call(bf16[2048,256]{1,0:T(8,128)(2,1)S(1)} %bitcast.12, bf16[2048,128]{1,0:T(8,128)(2,1)S(1)} %bitcast.13, ...), custom_call_target="tpu_custom_call" | custom-call | tf_op jit(solution)/shard_map/pallas_call | solution.py:1204
Async XLA Ops:
  0.6 77.7 %copy-start = (bf16[256,2048]{1,0:T(8,128)(2,1)S(1)}, bf16[256,2048]{1,0:T(8,128)(2,1)}, u32[]{:S(2)}) copy-start(bf16[256,2048]{1,0:T(8,128)(2,1)} %grad_out.1) | copy-start | bytes 3145732
  0.6 77.7 %copy-start.1 = (bf16[256,2048]{1,0:T(8,128)(2,1)S(1)}, bf16[256,2048]{1,0:T(8,128)(2,1)}, u32[]{:S(2)}) copy-start(bf16[256,2048]{1,0:T(8,128)(2,1)} %resid.1) | copy-start | bytes 3145732
  0.7 77.7 %copy-start.2 = (bf16[2048,128]{1,0:T(8,128)(2,1)S(1)}, bf16[2048,128]{1,0:T(8,128)(2,1)}, u32[]{:S(2)}) copy-start(bf16[2048,128]{1,0:T(8,128)(2,1)} %proj_weight.1) | copy-start | bytes 1572868
  0.7 77.7 %copy-start.3 = (bf16[256,128]{1,0:T(8,128)(2,1)S(1)}, bf16[256,128]{1,0:T(8,128)(2,1)}, u32[]{:S(2)}) copy-start(bf16[256,128]{1,0:T(8,128)(2,1)} %conv_sum.1) | copy-start | bytes 196612
  0.7 77.7 %copy-start.4 = (bf16[256,128]{1,0:T(8,128)(2,1)S(1)}, bf16[256,128]{1,0:T(8,128)(2,1)}, u32[]{:S(2)}) copy-start(bf16[256,128]{1,0:T(8,128)(2,1)} %conv_value.1) | copy-start | bytes 196612
  0.7 77.7 %copy-start.5 = (bf16[256,128]{1,0:T(8,128)(2,1)S(1)}, bf16[256,128]{1,0:T(8,128)(2,1)}, u32[]{:S(2)}) copy-start(bf16[256,128]{1,0:T(8,128)(2,1)} %conv_gate.1) | copy-start | bytes 196612
  0.7 77.7 %copy-start.6 = (f32[2048]{0:T(1024)S(1)}, f32[2048]{0:T(1024)}, u32[]{:S(2)}) copy-start(f32[2048]{0:T(1024)} %param.16) | copy-start | bytes 24580
  0.7 77.7 %copy-start.7 = (f32[31,128]{1,0:T(8,128)S(1)}, f32[31,128]{1,0:T(8,128)}, u32[]{:S(2)}) copy-start(f32[31,128]{1,0:T(8,128)} %conv_taps.1) | copy-start | bytes 47620
  0.7 77.7 %copy-start.8 = (f32[128]{0:T(128)S(1)}, f32[128]{0:T(128)}, u32[]{:S(2)}) copy-start(f32[128]{0:T(128)} %param.24) | copy-start | bytes 1540

commit v5 on v4

--- a/solution.py
+++ b/solution.py
@@ -393,17 +393,231 @@
     return codes
 
 
+def settle_body(
+    steps, meanwhile, part_grad, grad_out, resid, norm_gain, proj_weight,
+    conv_sum, conv_gain, conv_taps, conv_value, conv_gate,
+    side_out, feature_cols, proj, value_grad, gate_input_grad,
+    full, grads, extended, far_send, far_recv, near_send, near_recv, fwd_send, fwd_recv,
+    own_sem, x_send, x_recv, xf_send, xf_recv, xn_send, xn_recv, xw_send, xw_recv,
+    h_send, h_recv,
+):
+    s = lax.axis_index("sp")
+    t, near, far, diag = tp_places()
+    tok_rows, width = part_grad.shape
+    chunks, share = feature_cols.shape[1], feature_cols.shape[2]
+    feat_rows = feature_cols.shape[3]
+    overlap = conv_taps.shape[0] - 1
+
+    def rows_of(j):
+        return pl.ds(pl.multiple_of(j * share, share), share)
+
+    def lanes(q):
+        return pl.ds(pl.multiple_of(q * width, width), width)
+
+    def mine_at(j):
+        return full.at[rows_of(j), lanes(t)]
+
+    def own_copy():
+        return pltpu.make_async_copy(part_grad, full.at[:, lanes(t)], own_sem.at[0])
+
+    def gather(j, q, src, target, send_sem, recv_sem):
+        return pltpu.make_async_remote_copy(
+            src_ref=src,
+            dst_ref=full.at[rows_of(j), lanes(q)],
+            send_sem=send_sem.at[j],
+            recv_sem=recv_sem.at[j],
+            device_id=(s, target),
+            device_id_type=MESH,
+        )
+
+    def to_far(j):
+        return gather(j, t, part_grad.at[rows_of(j), :], far, far_send, far_recv)
+
+    def to_near(j):
+        return gather(j, t, part_grad.at[rows_of(j), :], near, near_send, near_recv)
+
+    def pass_near(j):
+        return gather(j, far, full.at[rows_of(j), lanes(far)], near, fwd_send, fwd_recv)
+
+    def spread_out(d):
+        feats = pl.ds(pl.multiple_of(((s + d) % steps) * feat_rows, feat_rows), feat_rows)
+        return pltpu.make_async_remote_copy(
+            src_ref=grads.at[rows_of(t), feats],
+            dst_ref=feature_cols.at[d, t],
+            send_sem=x_send.at[d],
+            recv_sem=x_recv.at[d],
+            device_id=((s + d) % steps, t),
+            device_id_type=MESH,
+        )
+
+    def beside(d, q, target, send_sem, recv_sem):
+        return pltpu.make_async_remote_copy(
+            src_ref=feature_cols.at[d, q],
+            dst_ref=feature_cols.at[d, q],
+            send_sem=send_sem.at[d],
+            recv_sem=recv_sem.at[d],
+            device_id=(s, target),
+            device_id_type=MESH,
+        )
+
+    def x_far(d):
+        return beside(d, t, far, xf_send, xf_recv)
+
+    def x_near(d):
+        return beside(d, t, near, xn_send, xn_recv)
+
+    def x_pass(d):
+        return beside(d, far, near, xw_send, xw_recv)
+
+    def halo():
+        return pltpu.make_async_remote_copy(
+            src_ref=extended.at[pl.ds(0, overlap + 2)],
+            dst_ref=extended.at[pl.ds(tok_rows, overlap + 2)],
+            send_sem=h_send.at[0],
+            recv_sem=h_recv.at[0],
+            device_id=((s + steps - 1) % steps, t),
+            device_id_type=MESH,
+        )
+
+    gain = norm_gain[...]
+
+    def settle(j):
+        here = rows_of(j)
+        feature_grad = full[here, :].astype(jnp.float32) * gain
+        x = resid[here, :].astype(jnp.float32)
+        scale = lax.rsqrt(jnp.mean(x * x, axis=-1, keepdims=True) + 1e-06)
+        cubed = scale * scale * scale
+        mean = jnp.mean(x * feature_grad, axis=-1, keepdims=True)
+        value = grad_out[here, :].astype(jnp.float32) + scale * feature_grad - x * cubed * mean
+        grads[here, :] = value.astype(grads.dtype)
+
+    def crossing(k):
+        return crossing_first(steps, k)
+
+    for j in (far, diag, t, near):
+        to_far(j).start()
+    for j in (near, t, diag, far):
+        to_near(j).start()
+    own_copy().start()
+    summed = conv_sum[...].astype(jnp.float32)
+    centre = summed - jnp.mean(summed, axis=-1, keepdims=True)
+    inv_std = lax.rsqrt(jnp.mean(centre * centre, axis=-1, keepdims=True) + 1e-05)
+    grouped = centre * inv_std
+    pre_act = grouped * conv_gain[...]
+    sigma = jax.nn.sigmoid(pre_act)
+    slope = sigma * (1.0 + pre_act * (1.0 - sigma)) * conv_gain[...]
+    own_copy().wait()
+
+    def arrive(j):
+        to_far(j).wait_recv()
+        pass_near(j).start()
+
+    def whole(j):
+        to_near(j).wait_recv()
+        pass_near(j).wait_recv()
+
+    arrive(t)
+    arrive(near)
+    whole(t)
+    settle(t)
+    looped(0, steps - 1, lambda k: spread_out(crossing(k)).start())
+    meanwhile()
+    arrive(far)
+    arrive(diag)
+    for j in (near, far, diag):
+        whole(j)
+        settle(j)
+    feats = pl.ds(pl.multiple_of(s * feat_rows, feat_rows), feat_rows)
+    feature_cols[0] = grads[:, feats].reshape(chunks, share, feat_rows)
+    out_grad = jnp.dot(grads[...], proj_weight[...], preferred_element_type=jnp.float32)
+    normal = out_grad * slope
+    sum_grad = inv_std * (
+        normal
+        - jnp.mean(normal, axis=-1, keepdims=True)
+        - grouped * jnp.mean(normal * grouped, axis=-1, keepdims=True)
+    )
+    extended[pl.ds(0, tok_rows), :] = sum_grad
+    halo().start()
+
+    def share_out(d):
+        spread_out(d).wait_recv()
+        x_far(d).start()
+        x_near(d).start()
+
+    def pass_on(d):
+        x_far(d).wait_recv()
+        x_pass(d).start()
+
+    def term(d):
+        left = feature_cols[d].reshape(tok_rows, feat_rows)
+        return contract_rows(left, side_out[d])
+
+    def gather_term(d):
+        x_near(d).wait_recv()
+        x_pass(d).wait_recv()
+        proj[...] += term(d)
+
+    def both(k):
+        share_out(crossing(k))
+        pass_on(crossing(k - 1))
+
+        @pl.when(k >= 2)
+        def _():
+            gather_term(crossing(k - 2))
+
+    proj[...] = term(0)
+    share_out(crossing(0))
+    looped(1, steps - 1, both)
+    halo().wait()
+
+    @pl.when(s == steps - 1)
+    def _():
+        extended[pl.ds(tok_rows, overlap + 2), :] = jnp.zeros(
+            (overlap + 2, extended.shape[1]), extended.dtype
+        )
+
+    gated_grad = extended[pl.ds(overlap, tok_rows), :] * conv_taps[pl.ds(0, 1), :]
+    for j in range(1, overlap + 1):
+        gated_grad += extended[pl.ds(overlap - j, tok_rows), :] * conv_taps[pl.ds(j, 1), :]
+    sigma_gate = jax.nn.sigmoid(conv_gate[...].astype(jnp.float32))
+    value_grad[...] = (gated_grad * sigma_gate).astype(value_grad.dtype)
+    gate_input_grad[...] = (
+        gated_grad * conv_value[...].astype(jnp.float32) * sigma_gate * (1.0 - sigma_gate)
+    ).astype(gate_input_grad.dtype)
+    pass_on(crossing(steps - 2))
+    gather_term(crossing(steps - 3))
+    gather_term(crossing(steps - 2))
+
+    def finish(k):
+        d = crossing(k)
+        spread_out(d).wait_send()
+        x_near(d).wait_send()
+        x_far(d).wait_send()
+        x_pass(d).wait_send()
+
+    looped(0, steps - 1, finish)
+
+    def finish_gather(j):
+        to_far(j).wait_send()
+        to_near(j).wait_send()
+        pass_near(j).wait_send()
+
+    looped(0, chunks, finish_gather)
+
+
 def relay_kernel(
     steps, routes_in, weights_in, grad_in, resid_in, gain_in, gate_in, up_in, down_in, sum_in,
-    conv_gain_in,
-    gate_grad, up_grad, down_grad, part_grad, side_out,
+    conv_gain_in, proj_in, taps_in, value_in, convgate_in,
+    gate_grad, up_grad, down_grad, proj, value_grad, gate_input_grad,
     routes, route_weights, grad_out, resid, norm_gain, w_gate, w_up, w_down, conv_sum, conv_gain,
-    normed, info, infos, ranks, weights, before, picks,
+    proj_weight, conv_taps, conv_value, conv_gate, part_grad, side_out, feature_cols, full, grads,
+    extended, normed, info, infos, ranks, weights, before, picks,
     tok, over, cross, cross_far, held, act, gate_pg, up_pg, part,
     near_in, pair, far_in, total, ret, side,
     own_sem, info_send, info_recv, line_send, line_recv, end_send, cross_recv,
     across_send, afar_send, arr_recv, b_send, f_send, c_send, near_recv, fwd_recv, far_recv,
     n0_send, n0_recv, n1_send, n1_recv, g_send, g_recv, r_send, r_recv, s_send, s_recv,
+    *settle_sems,
 ):
     s = lax.axis_index("sp")
     t, near, far, diag = tp_places()
@@ -445,6 +659,10 @@
                 (gate_in, w_gate),
                 (up_in, w_up),
                 (down_in, w_down),
+                (proj_in, proj_weight),
+                (taps_in, conv_taps),
+                (value_in, conv_value),
+                (convgate_in, conv_gate),
             )
         )
     ]
@@ -863,13 +1081,8 @@
             for a in both:
                 far_copy(a, j).wait_send()
 
-    looped(0, steps, finish)
-
     def finish_side(d):
-        side_copy(d).wait()
-
-    looped(1, steps, finish_side)
-    looped(1, line, lambda dz: info_copy(dz).wait_send())
+        side_copy(d).wait_send()
 
     def finish_line(m):
         for up in both:
@@ -886,15 +1099,26 @@
                     for col in both:
                         end_copy(a, zb, col, up).wait_send()
 
-    looped(0, line, finish_line)
-
     def finish_across(zb):
         for a in both:
             across_copy(a, zb).wait_send()
 
-    looped(0, line, finish_across)
-    for a in both:
-        across_far(a).wait_send()
+    def meanwhile():
+        looped(1, steps, lambda d: side_copy(d).wait_recv())
+        looped(0, steps, finish)
+        looped(1, steps, finish_side)
+        looped(1, line, lambda dz: info_copy(dz).wait_send())
+        looped(0, line, finish_line)
+        looped(0, line, finish_across)
+        for a in both:
+            across_far(a).wait_send()
+
+    settle_body(
+        steps, meanwhile, part_grad, grad_out, resid, norm_gain, proj_weight,
+        conv_sum, conv_gain, conv_taps, conv_value, conv_gate,
+        side_out, feature_cols, proj, value_grad, gate_input_grad,
+        full, grads, extended, *settle_sems,
+    )
 
 
 def relay_experts(operands, collective_id):
@@ -907,12 +1131,15 @@
     hidden = w_gate.shape[1]
     kind = resid.dtype
     block = (steps, count, width)
+    channels = conv_sum.shape[1]
+    tail_rows = conv_sum.shape[0] + operands[11].shape[0] + 1
     outs = [
         jax.ShapeDtypeStruct((model_width, hidden), kind),
         jax.ShapeDtypeStruct((model_width, hidden), kind),
         jax.ShapeDtypeStruct((hidden, model_width), kind),
-        jax.ShapeDtypeStruct((tok_rows, width), kind),
-        jax.ShapeDtypeStruct((steps,) + conv_sum.shape, kind),
+        jax.ShapeDtypeStruct((model_width // steps, channels), jnp.float32),
+        jax.ShapeDtypeStruct((tok_rows, channels), kind),
+        jax.ShapeDtypeStruct((tok_rows, channels), kind),
     ]
     held = pl.BlockSpec(memory_space=pltpu.VMEM)
     outside = pl.BlockSpec(memory_space=pltpu.HBM)
@@ -927,6 +1154,12 @@
         out_specs=tuple(held for _ in outs),
         scratch_shapes=[pltpu.VMEM(x.shape, x.dtype) for x in operands]
         + [
+            pltpu.VMEM((tok_rows, width), kind),
+            pltpu.VMEM((steps,) + conv_sum.shape, kind),
+            pltpu.VMEM((steps, tp_count, tok_rows // tp_count, model_width // steps), kind),
+            pltpu.VMEM((tok_rows, model_width), kind),
+            pltpu.VMEM((tok_rows, model_width), kind),
+            pltpu.VMEM((tail_rows, channels), jnp.float32),
             pltpu.VMEM((tok_rows, model_width), kind),
             pltpu.VMEM((2 * routes.shape[0], tok_rows), jnp.float32),
             pltpu.VMEM((line, 2 * routes.shape[0], tok_rows), jnp.float32),
@@ -947,268 +1180,35 @@
         + [sems(len(operands)), sems(line), sems(line), sems(2, 2, line), sems(2, line), sems(2, 2, line)]
         + [sems(2, line), sems(2, line), sems(2), sems(2, steps)]
         + [sems(2, steps)] * 6
-        + [sems(steps)] * 10,
+        + [sems(steps)] * 10
+        + [sems(tp_count)] * 6
+        + [sems(1)]
+        + [sems(steps)] * 8
+        + [sems(1)] * 2,
         compiler_params=pltpu.CompilerParams(
             collective_id=collective_id, has_side_effects=True, vmem_limit_bytes=42 << 20
         ),
     )(*(pltpu.with_memory_space_constraint(x, pltpu.HBM) for x in operands))
 
 
-def settle_kernel(
-    steps, part_grad, grad_out, resid, norm_gain, proj_weight,
-    conv_sum, conv_gain, conv_taps, conv_value, conv_gate,
-    feature_cols, value_grad, gate_input_grad,
-    full, grads, extended, far_send, far_recv, near_send, near_recv, fwd_send, fwd_recv,
-    own_sem, x_send, x_recv, xf_send, xf_recv, xn_send, xn_recv, xw_send, xw_recv,
-    h_send, h_recv,
-):
-    s = lax.axis_index("sp")
-    t, near, far, diag = tp_places()
-    tok_rows, width = part_grad.shape
-    chunks, share = feature_cols.shape[1], feature_cols.shape[2]
-    feat_rows = feature_cols.shape[3]
-    overlap = conv_taps.shape[0] - 1
-
-    def rows_of(j):
-        return pl.ds(pl.multiple_of(j * share, share), share)
-
-    def lanes(q):
-        return pl.ds(pl.multiple_of(q * width, width), width)
-
-    def mine_at(j):
-        return full.at[rows_of(j), lanes(t)]
-
-    def own_copy():
-        return pltpu.make_async_copy(part_grad, full.at[:, lanes(t)], own_sem.at[0])
-
-    def gather(j, q, src, target, send_sem, recv_sem):
-        return pltpu.make_async_remote_copy(
-            src_ref=src,
-            dst_ref=full.at[rows_of(j), lanes(q)],
-            send_sem=send_sem.at[j],
-            recv_sem=recv_sem.at[j],
-            device_id=(s, target),
-            device_id_type=MESH,
-        )
-
-    def to_far(j):
-        return gather(j, t, part_grad.at[rows_of(j), :], far, far_send, far_recv)
-
-    def to_near(j):
-        return gather(j, t, part_grad.at[rows_of(j), :], near, near_send, near_recv)
-
-    def pass_near(j):
-        return gather(j, far, full.at[rows_of(j), lanes(far)], near, fwd_send, fwd_recv)
-
-    def spread_out(d):
-        feats = pl.ds(pl.multiple_of(((s + d) % steps) * feat_rows, feat_rows), feat_rows)
-        return pltpu.make_async_remote_copy(
-            src_ref=grads.at[rows_of(t), feats],
-            dst_ref=feature_cols.at[d, t],
-            send_sem=x_send.at[d],
-            recv_sem=x_recv.at[d],
-            device_id=((s + d) % steps, t),
-            device_id_type=MESH,
-        )
-
-    def beside(d, q, target, send_sem, recv_sem):
-        return pltpu.make_async_remote_copy(
-            src_ref=feature_cols.at[d, q],
-            dst_ref=feature_cols.at[d, q],
-            send_sem=send_sem.at[d],
-            recv_sem=recv_sem.at[d],
-            device_id=(s, target),
-            device_id_type=MESH,
-        )
-
-    def x_far(d):
-        return beside(d, t, far, xf_send, xf_recv)
-
-    def x_near(d):
-        return beside(d, t, near, xn_send, xn_recv)
-
-    def x_pass(d):
-        return beside(d, far, near, xw_send, xw_recv)
-
-    def halo():
-        return pltpu.make_async_remote_copy(
-            src_ref=extended.at[pl.ds(0, overlap + 2)],
-            dst_ref=extended.at[pl.ds(tok_rows, overlap + 2)],
-            send_sem=h_send.at[0],
-            recv_sem=h_recv.at[0],
-            device_id=((s + steps - 1) % steps, t),
-            device_id_type=MESH,
-        )
-
-    gain = norm_gain[...]
-
-    def settle(j):
-        here = rows_of(j)
-        feature_grad = full[here, :].astype(jnp.float32) * gain
-        x = resid[here, :].astype(jnp.float32)
-        scale = lax.rsqrt(jnp.mean(x * x, axis=-1, keepdims=True) + 1e-06)
-        cubed = scale * scale * scale
-        mean = jnp.mean(x * feature_grad, axis=-1, keepdims=True)
-        value = grad_out[here, :].astype(jnp.float32) + scale * feature_grad - x * cubed * mean
-        grads[here, :] = value.astype(grads.dtype)
-
-    def crossing(k):
-        return crossing_first(steps, k)
-
-    meet(steps, True, near, far)
-    for j in (far, diag, t, near):
-        to_far(j).start()
-    for j in (near, t, diag, far):
-        to_near(j).start()
-    own_copy().start()
-    summed = conv_sum[...].astype(jnp.float32)
-    centre = summed - jnp.mean(summed, axis=-1, keepdims=True)
-    inv_std = lax.rsqrt(jnp.mean(centre * centre, axis=-1, keepdims=True) + 1e-05)
-    grouped = centre * inv_std
-    pre_act = grouped * conv_gain[...]
-    sigma = jax.nn.sigmoid(pre_act)
-    slope = sigma * (1.0 + pre_act * (1.0 - sigma)) * conv_gain[...]
-    own_copy().wait()
-
-    def arrive(j):
-        to_far(j).wait_recv()
-        pass_near(j).start()
-
-    def whole(j):
-        to_near(j).wait_recv()
-        pass_near(j).wait_recv()
-
-    arrive(t)
-    arrive(near)
-    whole(t)
-    settle(t)
-    looped(0, steps - 1, lambda k: spread_out(crossing(k)).start())
-    arrive(far)
-    arrive(diag)
-    for j in (near, far, diag):
-        whole(j)
-        settle(j)
-    feats = pl.ds(pl.multiple_of(s * feat_rows, feat_rows), feat_rows)
-    feature_cols[0] = grads[:, feats].reshape(chunks, share, feat_rows)
-    out_grad = jnp.dot(grads[...], proj_weight[...], preferred_element_type=jnp.float32)
-    normal = out_grad * slope
-    sum_grad = inv_std * (
-        normal
-        - jnp.mean(normal, axis=-1, keepdims=True)
-        - grouped * jnp.mean(normal * grouped, axis=-1, keepdims=True)
-    )
-    extended[pl.ds(0, tok_rows), :] = sum_grad
-    halo().start()
-
-    def share_out(d):
-        spread_out(d).wait_recv()
-        x_far(d).start()
-        x_near(d).start()
-
-    def pass_on(d):
-        x_far(d).wait_recv()
-        x_pass(d).start()
-
-    def both(k):
-        share_out(crossing(k))
-        pass_on(crossing(k - 1))
-
-    share_out(crossing(0))
-    looped(1, steps - 1, both)
-    halo().wait()
-
-    @pl.when(s == steps - 1)
-    def _():
-        extended[pl.ds(tok_rows, overlap + 2), :] = jnp.zeros(
-            (overlap + 2, extended.shape[1]), extended.dtype
-        )
-
-    gated_grad = extended[pl.ds(overlap, tok_rows), :] * conv_taps[pl.ds(0, 1), :]
-    for j in range(1, overlap + 1):
-        gated_grad += extended[pl.ds(overlap - j, tok_rows), :] * conv_taps[pl.ds(j, 1), :]
-    sigma_gate = jax.nn.sigmoid(conv_gate[...].astype(jnp.float32))
-    value_grad[...] = (gated_grad * sigma_gate).astype(value_grad.dtype)
-    gate_input_grad[...] = (
-        gated_grad * conv_value[...].astype(jnp.float32) * sigma_gate * (1.0 - sigma_gate)
-    ).astype(gate_input_grad.dtype)
-    pass_on(crossing(steps - 2))
-
-    def finish(k):
-        d = crossing(k)
-        spread_out(d).wait_send()
-        x_near(d).wait()
-        x_far(d).wait_send()
-        x_pass(d).wait()
-
-    looped(0, steps - 1, finish)
-
-    def finish_gather(j):
-        to_far(j).wait_send()
-        to_near(j).wait_send()
-        pass_near(j).wait_send()
-
-    looped(0, chunks, finish_gather)
-
-
-def settle_tokens(operands, collective_id):
-    part_grad, resid, conv_sum = operands[0], operands[2], operands[5]
-    overlap = operands[7].shape[0] - 1
-    steps, tp_count = lax.axis_size("sp"), lax.axis_size("tp")
-    tok_rows, model_width = resid.shape
-    channels = conv_sum.shape[1]
-    kind = resid.dtype
-    outs = [
-        jax.ShapeDtypeStruct((steps, tp_count, tok_rows // tp_count, model_width // steps), kind),
-        jax.ShapeDtypeStruct((tok_rows, channels), kind),
-        jax.ShapeDtypeStruct((tok_rows, channels), kind),
-    ]
-    fours = pltpu.SemaphoreType.DMA((tp_count,))
-    ones = pltpu.SemaphoreType.DMA((steps,))
-    single = pltpu.SemaphoreType.DMA((1,))
-    return pl.pallas_call(
-        functools.partial(settle_kernel, steps),
-        out_shape=tuple(outs),
-        in_specs=[pl.BlockSpec(memory_space=pltpu.VMEM)] * len(operands),
-        out_specs=tuple(pl.BlockSpec(memory_space=pltpu.VMEM) for _ in outs),
-        scratch_shapes=[
-            pltpu.VMEM((tok_rows, model_width), kind),
-            pltpu.VMEM((tok_rows, model_width), kind),
-            pltpu.VMEM((tok_rows + overlap + 2, channels), jnp.float32),
-        ]
-        + [fours] * 6
-        + [single]
-        + [ones] * 8
-        + [single] * 2,
-        compiler_params=pltpu.CompilerParams(
-            collective_id=collective_id, has_side_effects=True, vmem_limit_bytes=24 << 20
-        ),
-    )(*operands)
-
-
-def last_kernel(count, feature_cols, all_out, *refs):
-    ins, proj, outs, sem = refs[:count], refs[count], refs[count + 1 : -1], refs[-1]
+def last_kernel(count, *refs):
+    ins, outs, sem = refs[:count], refs[count:-1], refs[-1]
     moves = [pltpu.make_async_copy(a, b, sem.at[i]) for i, (a, b) in enumerate(zip(ins, outs))]
     for move in moves:
         move.start()
-    proj[...] = contract_rows(feature_cols[...], all_out[...])
     for move in moves:
         move.wait()
 
 
-def last_stage(feature_cols, all_out, grads):
-    held = [pl.BlockSpec(memory_space=pltpu.VMEM)]
-    outside = [pl.BlockSpec(memory_space=pl.ANY)]
-    shape = (feature_cols.shape[1], all_out.shape[1])
-    outs = [jax.ShapeDtypeStruct(shape, jnp.float32)]
-    outs += [jax.ShapeDtypeStruct(g.shape, g.dtype) for g in grads]
+def last_stage(results):
     return pl.pallas_call(
-        functools.partial(last_kernel, len(grads)),
-        out_shape=tuple(outs),
-        in_specs=held * (2 + len(grads)),
-        out_specs=tuple(held + outside * len(grads)),
-        scratch_shapes=[pltpu.SemaphoreType.DMA((len(grads),))],
+        functools.partial(last_kernel, len(results)),
+        out_shape=tuple(jax.ShapeDtypeStruct(x.shape, x.dtype) for x in results),
+        in_specs=[pl.BlockSpec(memory_space=pltpu.VMEM)] * len(results),
+        out_specs=tuple(pl.BlockSpec(memory_space=pl.ANY) for _ in results),
+        scratch_shapes=[pltpu.SemaphoreType.DMA((len(results),))],
         compiler_params=pltpu.CompilerParams(vmem_limit_bytes=16 << 20),
-    )(feature_cols, all_out, *grads)
+    )(*results)
 
 
 def local(
@@ -1246,27 +1246,13 @@
             down_weight[0],
             conv_sum,
             conv_gain[None],
-        )
-        gate_grad, up_grad, down_grad, part_grad, all_out = relay_experts(operands, 4)
-        operands = (
-            part_grad,
-            grad_out,
-            resid,
-            norm_gain[None],
             proj_weight,
-            conv_sum,
-            conv_gain[None],
             conv_taps,
             conv_value,
             conv_gate,
         )
-        feature_cols, value_grad, gate_input_grad = settle_tokens(operands, 5)
-        proj_grad, *ends = last_stage(
-            feature_cols.reshape(sp_count * tok_rows, model_width // sp_count),
-            all_out.reshape(sp_count * tok_rows, channels),
-            (gate_grad, up_grad, down_grad, value_grad, gate_input_grad),
-        )
-        return tuple(g[None] for g in ends[:3]) + (proj_grad,) + tuple(ends[3:])
+        gate_grad, up_grad, down_grad, *rest = last_stage(relay_experts(operands, 4))
+        return (gate_grad[None], up_grad[None], down_grad[None], *rest)
     resid_f = resid.astype(jnp.float32)
     inv_rms = lax.rsqrt(jnp.mean(resid_f * resid_f, axis=-1, keepdims=True) + 1e-06)
     normed = (resid_f * inv_rms * norm_gain).astype(jnp.bfloat16)

time: 107 us -> 107 us (level)
    pallas_call x2 -> x1, Pallas kernels: 28.4 us -> 2.3 us  [last_stage(): pl.pallas_call(functools.partial(last_kernel, len(results)), out_shape=tu...]
    pallas_call x1, Pallas kernels: 77.6 us -> 104 us  [relay_experts(): pl.pallas_call(functools.partial(relay_kernel, steps), out_shape=tuple(ou...]
where the time goes in v5:
time: 107 us
  Pallas kernels  106 us (99%)
    pallas_call x1, Pallas kernels, relay_experts(): pl.pallas_call(functools.partial(relay_kernel, steps), out_shape=tuple(ou...  104 us
    pallas_call x1, Pallas kernels, last_stage(): pl.pallas_call(functools.partial(last_kernel, len(results)), out_shape=tu...  2.3 us

profile of v5, /device:TPU:0, one launch (start us, length us, event | category | flops | bytes accessed | tf_op | source)
XLA Modules:
  0.0 106.5 jit_solution(16408444605315031340)
XLA Ops:
  0.6 103.6 %shard_map.181 = (bf16[2048,384]{1,0:T(8,128)(2,1)S(1)}, bf16[2048,384]{1,0:T(8,128)(2,1)S(1)}, bf16[384,2048]{1,0:T(8,128)(2,1)S(1)}, f32[256,128]{1,0:T(8,128)...) custom-call(s32[2,256]{1,0:T(2,128)} %bitcast.14, f32[2,256]{1,0:T(2,128)} %bitcast.15, ...), custom_call_target="tpu_custom_call" | custom-call | tf_op jit(solution)/shard_map/pallas_call | solution.py:1150
  104.2 2.3 %shard_map.182 = (bf16[2048,384]{1,0:T(8,128)(2,1)}, bf16[2048,384]{1,0:T(8,128)(2,1)}, bf16[384,2048]{1,0:T(8,128)(2,1)}, f32[256,128]{1,0:T(8,128)}, bf16[256,...) custom-call(bf16[2048,384]{1,0:T(8,128)(2,1)S(1)} %get-tuple-element.18.refs_0_, ...), custom_call_target="tpu_custom_call" | custom-call | tf_op jit(solution)/shard_map/pallas_call | solution.py:1204

commit v6 on v5

--- a/solution.py
+++ b/solution.py
@@ -557,17 +557,9 @@
         x_pass(d).wait_recv()
         proj[...] += term(d)
 
-    def both(k):
-        share_out(crossing(k))
-        pass_on(crossing(k - 1))
-
-        @pl.when(k >= 2)
-        def _():
-            gather_term(crossing(k - 2))
-
     proj[...] = term(0)
-    share_out(crossing(0))
-    looped(1, steps - 1, both)
+    looped(0, steps - 1, lambda k: share_out(crossing(k)))
+    looped(0, steps - 1, lambda k: pass_on(crossing(k)))
     halo().wait()
 
     @pl.when(s == steps - 1)
@@ -584,9 +576,7 @@
     gate_input_grad[...] = (
         gated_grad * conv_value[...].astype(jnp.float32) * sigma_gate * (1.0 - sigma_gate)
     ).astype(gate_input_grad.dtype)
-    pass_on(crossing(steps - 2))
-    gather_term(crossing(steps - 3))
-    gather_term(crossing(steps - 2))
+    looped(0, steps - 1, lambda k: gather_term(crossing(k)))
 
     def finish(k):
         d = crossing(k)
@@ -1029,15 +1019,18 @@
             looped(1, steps, lambda d: side_copy(d).start())
 
         forward(j)
-        experts(j)
-
-        @pl.when(n == 0)
-        def _():
-            add_pair(j)
-
-        @pl.when(n > middle)
-        def _():
-            add_pair(chunk_at(n - 1))
+
+        @pl.when(n >= 1)
+        def _():
+            experts(chunk_at(n - 1))
+
+        @pl.when(n == 1)
+        def _():
+            add_pair(chunk_at(0))
+
+        @pl.when(n > middle + 1)
+        def _():
+            add_pair(chunk_at(n - 2))
 
     def pair_at(n):
         add_pair(chunk_at(n))
@@ -1047,15 +1040,19 @@
 
     looped(0, steps, slot)
     half = model_width // 512
+    experts(chunk_at(steps - 1))
+    add_pair(chunk_at(steps - 2))
     pair_at(steps - 1)
     looped(1, middle, pair_at)
     looped(middle, steps - 2, back_at)
-    looped(0, half, row_grads)
+    looped(0, half // 2, row_grads)
     back_at(steps - 2)
-    looped(half, 2 * half, row_grads)
+    looped(half // 2, half, row_grads)
     back_at(steps - 1)
+    looped(half, half + half // 2, row_grads)
+    looped(1, middle, back_at)
+    looped(half + half // 2, 2 * half, row_grads)
     looped(0, half, act_grads)
-    looped(1, middle, back_at)
     back_at(0)
 
     def gather_back(d):

time: 107 us -> 98.2 us (0.918)
  Pallas kernels: 106 us -> 96.8 us
    pallas_call x1, Pallas kernels: 104 us -> 94.5 us  [relay_experts(): pl.pallas_call(functools.partial(relay_kernel, steps), out_shape=tuple(ou...]
where the time goes in v6:
time: 98.2 us; the launch traced here: 97.4 us
  Pallas kernels  96.8 us (99%)
    pallas_call x1, Pallas kernels, relay_experts(): pl.pallas_call(functools.partial(relay_kernel, steps), out_shape=tuple(ou...  94.5 us
    pallas_call x1, Pallas kernels, last_stage(): pl.pallas_call(functools.partial(last_kernel, len(results)), out_shape=tu...  2.3 us

profile of v6, /device:TPU:0, one launch (start us, length us, event | category | flops | bytes accessed | tf_op | source)
XLA Modules:
  0.0 97.4 jit_solution(11707332960942909763)
XLA Ops:
  0.6 94.5 %shard_map.181 = (bf16[2048,384]{1,0:T(8,128)(2,1)S(1)}, bf16[2048,384]{1,0:T(8,128)(2,1)S(1)}, bf16[384,2048]{1,0:T(8,128)(2,1)S(1)}, f32[256,128]{1,0:T(8,128)...) custom-call(s32[2,256]{1,0:T(2,128)} %bitcast.14, f32[2,256]{1,0:T(2,128)} %bitcast.15, ...), custom_call_target="tpu_custom_call" | custom-call | tf_op jit(solution)/shard_map/pallas_call | solution.py:1147
  95.1 2.3 %shard_map.182 = (bf16[2048,384]{1,0:T(8,128)(2,1)}, bf16[2048,384]{1,0:T(8,128)(2,1)}, bf16[384,2048]{1,0:T(8,128)(2,1)}, f32[256,128]{1,0:T(8,128)}, bf16[256,...) custom-call(bf16[2048,384]{1,0:T(8,128)(2,1)S(1)} %get-tuple-element.18.refs_0_, ...), custom_call_target="tpu_custom_call" | custom-call | tf_op jit(solution)/shard_map/pallas_call | solution.py:1201

commit v7 on v6

--- a/solution.py
+++ b/solution.py
@@ -494,7 +494,7 @@
     def crossing(k):
         return crossing_first(steps, k)
 
-    for j in (far, diag, t, near):
+    for j in (diag, far, t, near):
         to_far(j).start()
     for j in (near, t, diag, far):
         to_near(j).start()
@@ -516,8 +516,8 @@
         to_near(j).wait_recv()
         pass_near(j).wait_recv()
 
+    arrive(near)
     arrive(t)
-    arrive(near)
     whole(t)
     settle(t)
     looped(0, steps - 1, lambda k: spread_out(crossing(k)).start())
@@ -795,8 +795,8 @@
         def _():
             arrival(a, j).wait_recv()
             end_copy(a, zb, 1, up).wait_recv()
+            share(a, j)
             across_copy(a, zb).start()
-            share(a, j)
 
         @pl.when(valid(m, up) & jnp.logical_not(at_end(up)))
         def _():
@@ -810,10 +810,10 @@
             def _():
                 line_copy(a, zb, tok.at[a, zb], up).start()
 
+            held[a, j, :, lanes(t)] = selected(a, zb, s, tok[a, zb])
+            share(a, j)
             cross[a, zb] = selected(a, zb, across, tok[a, zb])
             across_copy(a, zb).start()
-            held[a, j, :, lanes(t)] = selected(a, zb, s, tok[a, zb])
-            share(a, j)
 
     def unless_own(j, body):
         @pl.when(j != s)

time: 98.2 us -> 98 us (level)
  no operation moved by 1% of the time
where the time goes in v7:
time: 98 us; the launch traced here: 97.9 us
  Pallas kernels  97.2 us (99%)
    pallas_call x1, Pallas kernels, relay_experts(): pl.pallas_call(functools.partial(relay_kernel, steps), out_shape=tuple(ou...  95 us
    pallas_call x1, Pallas kernels, last_stage(): pl.pallas_call(functools.partial(last_kernel, len(results)), out_shape=tu...  2.3 us

profile of v7, /device:TPU:0, one launch (start us, length us, event | category | flops | bytes accessed | tf_op | source)
XLA Modules:
  0.0 97.9 jit_solution(14599546055132770295)
XLA Ops:
  0.6 95.0 %shard_map.181 = (bf16[2048,384]{1,0:T(8,128)(2,1)S(1)}, bf16[2048,384]{1,0:T(8,128)(2,1)S(1)}, bf16[384,2048]{1,0:T(8,128)(2,1)S(1)}, f32[256,128]{1,0:T(8,128)...) custom-call(s32[2,256]{1,0:T(2,128)} %bitcast.14, f32[2,256]{1,0:T(2,128)} %bitcast.15, ...), custom_call_target="tpu_custom_call" | custom-call | tf_op jit(solution)/shard_map/pallas_call | solution.py:1147
  95.6 2.3 %shard_map.182 = (bf16[2048,384]{1,0:T(8,128)(2,1)}, bf16[2048,384]{1,0:T(8,128)(2,1)}, bf16[384,2048]{1,0:T(8,128)(2,1)}, f32[256,128]{1,0:T(8,128)}, bf16[256,...) custom-call(bf16[2048,384]{1,0:T(8,128)(2,1)S(1)} %get-tuple-element.18.refs_0_, ...), custom_call_target="tpu_custom_call" | custom-call | tf_op jit(solution)/shard_map/pallas_call | solution.py:1201
